TPU v7x, 256 devices: a whole 4x4x8 slice. The times are simulated.
256 devices in a mesh: kv: 32 (over z, y), tp: 8 (over x, core).
Axes of the slice: x: 4, y: 4, z: 8, core: 2. Of those that a mesh axis runs over, the one named last changes fastest.
Arguments:
- residual: bfloat16 [1024, 2048], P('kv', 'tp'), may hold values from -12 to 12
- first_gain: bfloat16 [2048], P('tp'), may hold values from 0.099609375 to 1.8984375
- first_gate: bfloat16 [2048, 5632], P('tp', 'kv'), may hold values from -0.125 to 0.125
- first_lift: bfloat16 [2048, 5632], P('tp', 'kv'), may hold values from -0.125 to 0.125
- first_down: bfloat16 [5632, 2048], P('kv', 'tp'), may hold values from -0.078125 to 0.078125
- mixer_gain: bfloat16 [2048], replicated, may hold values from 0.099609375 to 1.8984375
- proj_gate: bfloat16 [2048, 2048], P(None, 'tp'), may hold values from -0.125 to 0.125
- proj_input: bfloat16 [2048, 2048], P(None, 'tp'), may hold values from -0.125 to 0.125
- proj_write: bfloat16 [2048, 1024], P(None, 'tp'), may hold values from -0.125 to 0.125
- proj_read: bfloat16 [2048, 1024], P(None, 'tp'), may hold values from -0.125 to 0.125
- proj_step: bfloat16 [2048, 32], P(None, 'tp'), may hold values from -0.125 to 0.125
- step_bias: float32 [32], P('tp'), may hold values from -5 to -2
- rate_log: float32 [32], P('tp'), may hold values from -0.7 to 2.1
- skip_gain: float32 [32], P('tp'), may hold values from 0.5 to 2
- taps_input: bfloat16 [4, 2048], P(None, 'tp'), may hold values from -3 to 3
- taps_write: bfloat16 [4, 1024], P(None, 'tp'), may hold values from -3 to 3
- taps_read: bfloat16 [4, 1024], P(None, 'tp'), may hold values from -3 to 3
- buffer_input: bfloat16 [1024, 3, 2048], P('kv', None, 'tp'), may hold values from -6 to 6
- buffer_write: bfloat16 [1024, 3, 1024], P('kv', None, 'tp'), may hold values from -6 to 6
- buffer_read: bfloat16 [1024, 3, 1024], P('kv', None, 'tp'), may hold values from -6 to 6
- scan_state: float32 [1024, 32, 64, 128], P('kv', 'tp'), may hold values from -1.5 to 1.5
- group_gain: bfloat16 [2048], P('tp'), may hold values from 0.099609375 to 1.8984375
- proj_output: bfloat16 [2048, 2048], P('tp'), may hold values from -0.125 to 0.125
- second_gain: bfloat16 [2048], P('tp'), may hold values from 0.099609375 to 1.8984375
- second_gate: bfloat16 [2048, 5632], P('tp', 'kv'), may hold values from -0.125 to 0.125
- second_lift: bfloat16 [2048, 5632], P('tp', 'kv'), may hold values from -0.125 to 0.125
- second_down: bfloat16 [5632, 2048], P('kv', 'tp'), may hold values from -0.078125 to 0.078125
Outputs:
- residual_out: bfloat16 [1024, 2048], P('kv', 'tp')
- state_out: float32 [1024, 32, 64, 128], P('kv', 'tp')
All inputs are finite; a program needn't handle non-finite values.
Results may differ from a plain program's by a relative error of at most 0.023.
Values may be sent and summed in bfloat16 or wider, within the bound.
A program may use at most 64 MiB of HBM per device.

v0:
```python
import jax
import jax.numpy as jnp
from jax import lax
from jax.sharding import PartitionSpec as P

D = 2048
HEAD_DIM = 64
STATE = 128


norm_eps = 1e-06


def sent_to_all(array, axis):
    length = lax.axis_size(axis)
    return lax.all_to_all(
        jnp.broadcast_to(array[None], (length, *array.shape)), axis, 0, 0, tiled=True
    )


def over_copies(array, axis):
    everything = sent_to_all(array, axis)
    return jnp.sum(everything, axis=0)


def joined_along(tiles, dim):
    tiles = jnp.moveaxis(tiles, 0, dim)
    shape = tiles.shape
    return tiles.reshape(*shape[:dim], shape[dim] * shape[dim + 1], *shape[dim + 2 :])


def gathered_copies(array, axis, dim):
    return joined_along(sent_to_all(array, axis), dim)


def in_blocks(array, dim, length):
    before, after = (array.shape[:dim], array.shape[dim + 1 :])
    return jnp.moveaxis(array.reshape(*before, length, -1, *after), dim, 0)


def sum_at_owner(array, axis, dim):
    length = lax.axis_size(axis)
    tiles = lax.all_to_all(in_blocks(array, dim, length), axis, 0, 0, tiled=True)
    return jnp.sum(tiles.astype(jnp.float32), axis=0)


def inverse_rms(values):
    return lax.rsqrt(jnp.mean(values * values, axis=-1, keepdims=True) + norm_eps)


def half_step(residual, gain, gate_weight, lift_weight, down_weight):
    widened = residual.astype(jnp.float32)
    row_total = over_copies(jnp.sum(widened * widened, axis=1), "tp")
    factor = lax.rsqrt(row_total / D + norm_eps)
    normed = (widened * factor[:, None] * gain.astype(jnp.float32)[None, :]).astype(jnp.bfloat16)
    hidden_cols = gate_weight.shape[1]
    row_piece = gathered_copies(normed, "kv", 0)
    gate_part = jnp.dot(row_piece, gate_weight, preferred_element_type=jnp.float32).astype(
        jnp.bfloat16
    )
    lift_part = jnp.dot(row_piece, lift_weight, preferred_element_type=jnp.float32).astype(
        jnp.bfloat16
    )
    joined = lax.optimization_barrier(jnp.concatenate([gate_part, lift_part], axis=1))
    partial_value = joined.astype(jnp.float32)
    share = sum_at_owner(partial_value.astype(jnp.bfloat16), "tp", 0)
    active = (jax.nn.silu(share[:, :hidden_cols]) * share[:, hidden_cols:]).astype(jnp.bfloat16)
    hidden = gathered_copies(active, "tp", 0)
    branch = sum_at_owner(
        jnp.dot(hidden, down_weight, preferred_element_type=jnp.float32).astype(jnp.bfloat16),
        "kv",
        0,
    )
    return (widened + 0.5 * branch).astype(jnp.bfloat16)


def short_conv(tap_weights, buffer, newest):
    taps_f = tap_weights.astype(jnp.float32)
    summed = jnp.sum(buffer.astype(jnp.float32) * taps_f[None, :-1, :], axis=1)
    summed = summed + newest.astype(jnp.float32) * taps_f[-1][None, :]
    return jax.nn.silu(summed)


def state_mixer(
    residual,
    mixer_gain,
    proj_gate,
    proj_input,
    proj_write,
    proj_read,
    proj_step,
    step_bias,
    rate_log,
    skip_gain,
    taps_input,
    taps_write,
    taps_read,
    buffer_input,
    buffer_write,
    buffer_read,
    scan_state,
    group_gain,
    proj_output,
):
    seq_rows = residual.shape[0]
    full_rows = gathered_copies(residual, "tp", 1)
    widened = full_rows.astype(jnp.float32)
    normed = (widened * inverse_rms(widened) * mixer_gain.astype(jnp.float32)[None, :]).astype(
        jnp.bfloat16
    )

    def state_project(weight):
        return jnp.dot(normed, weight, preferred_element_type=jnp.float32).astype(jnp.bfloat16)

    gate_z = state_project(proj_gate)
    input_new = state_project(proj_input)
    write_new = state_project(proj_write)
    read_new = state_project(proj_read)
    step_raw = state_project(proj_step)
    input_conv = short_conv(taps_input, buffer_input, input_new)
    write_conv = short_conv(taps_write, buffer_write, write_new)
    read_conv = short_conv(taps_read, buffer_read, read_new)
    head_count = proj_step.shape[1]
    group_count = proj_write.shape[1] // STATE
    per_group = head_count // group_count
    step = jax.nn.softplus(step_raw.astype(jnp.float32) + step_bias[None, :])
    retain = jnp.exp(-step * jnp.exp(rate_log)[None, :])
    input_heads = input_conv.reshape(seq_rows, group_count, per_group, HEAD_DIM)
    write_groups = write_conv.reshape(seq_rows, group_count, STATE)
    read_groups = read_conv.reshape(seq_rows, group_count, STATE)
    old_state = scan_state.reshape(seq_rows, group_count, per_group, HEAD_DIM, STATE)
    retain_g = retain.reshape(seq_rows, group_count, per_group)
    step_g = step.reshape(seq_rows, group_count, per_group)
    updated = (
        retain_g[..., None, None] * old_state
        + (step_g[..., None] * input_heads)[..., None] * write_groups[:, :, None, None, :]
    )
    head_out = jnp.einsum("bgrpn,bgn->bgrp", updated, read_groups)
    head_out = head_out + skip_gain.reshape(group_count, per_group)[None, :, :, None] * input_heads
    head_short = lax.optimization_barrier(head_out.astype(jnp.bfloat16))
    gated = head_short.astype(jnp.float32).reshape(seq_rows, group_count, per_group * HEAD_DIM)
    gated = gated * jax.nn.silu(
        gate_z.astype(jnp.float32).reshape(seq_rows, group_count, per_group * HEAD_DIM)
    )
    gated = (
        gated
        * inverse_rms(gated)
        * group_gain.astype(jnp.float32).reshape(group_count, per_group * HEAD_DIM)[None]
    )
    gated = gated.reshape(seq_rows, head_count * HEAD_DIM).astype(jnp.bfloat16)
    partial_out = jnp.dot(gated, proj_output, preferred_element_type=jnp.float32).astype(
        jnp.bfloat16
    )
    partial_out = lax.optimization_barrier(partial_out).astype(jnp.float32)
    mixed = sum_at_owner(partial_out.astype(jnp.bfloat16), "tp", 1)
    mixed_rows = (residual.astype(jnp.float32) + mixed).astype(jnp.bfloat16)
    return (mixed_rows, updated.reshape(seq_rows, head_count, HEAD_DIM, STATE))


def per_device(
    residual,
    first_gain,
    first_gate,
    first_lift,
    first_down,
    mixer_gain,
    proj_gate,
    proj_input,
    proj_write,
    proj_read,
    proj_step,
    step_bias,
    rate_log,
    skip_gain,
    taps_input,
    taps_write,
    taps_read,
    buffer_input,
    buffer_write,
    buffer_read,
    scan_state,
    group_gain,
    proj_output,
    second_gain,
    second_gate,
    second_lift,
    second_down,
):
    first = half_step(residual, first_gain, first_gate, first_lift, first_down)
    mixed, state_out = state_mixer(
        first,
        mixer_gain,
        proj_gate,
        proj_input,
        proj_write,
        proj_read,
        proj_step,
        step_bias,
        rate_log,
        skip_gain,
        taps_input,
        taps_write,
        taps_read,
        buffer_input,
        buffer_write,
        buffer_read,
        scan_state,
        group_gain,
        proj_output,
    )
    residual_out = half_step(mixed, second_gain, second_gate, second_lift, second_down)
    return (residual_out, state_out)


def solution(mesh):
    placed = (
        P("kv", "tp"),
        P("tp"),
        P("tp", "kv"),
        P("tp", "kv"),
        P("kv", "tp"),
        P(),
        P(None, "tp"),
        P(None, "tp"),
        P(None, "tp"),
        P(None, "tp"),
        P(None, "tp"),
        P("tp"),
        P("tp"),
        P("tp"),
        P(None, "tp"),
        P(None, "tp"),
        P(None, "tp"),
        P("kv", None, "tp"),
        P("kv", None, "tp"),
        P("kv", None, "tp"),
        P("kv", "tp", None, None),
        P("tp"),
        P("tp", None),
        P("tp"),
        P("tp", "kv"),
        P("tp", "kv"),
        P("kv", "tp"),
    )
    return jax.shard_map(
        per_device,
        mesh=mesh,
        in_specs=placed,
        out_specs=(P("kv", "tp"), P("kv", "tp", None, None)),
        check_vma=False,
    )
```

profile of v0, /device:TPU:1, one launch (start us, length us, event | category | flops | bytes accessed | tf_op | source)
XLA Modules:
  0.0 203.2 jit_solution(12820025739309025349)
XLA Ops:
  0.6 0.0 copy-start
  0.6 0.9 fusion.19
  1.6 0.6 broadcast_in_dim.14
  2.2 6.4 %all-to-all-start = ((f32[8,1,32]{2,1,0:T(1,128)}), f32[8,1,32]{2,1,0:T(1,128)S(1)}, u32[]{:S(2)}, u32[]{:S(2)}) async-start(f32[8,1,32]{2,1,0:T(1,128)} %broadcast_in_dim.14), calls=%async_computation | async-start | bytes 8192 | tf_op jit(solution)/shard_map/all_to_all | solution.py:16
  8.6 0.7 convert_element_type.159
  9.2 3.9 %all-to-all-done = f32[8,1,32]{2,1,0:T(1,128)S(1)} async-done(((f32[8,1,32]{2,1,0:T(1,128)}), f32[8,1,32]{2,1,0:T(1,128)S(1)}, u32[]{:S(2)}, u32[]{:S(2)}) %all-to-all-start) | async-done | bytes 1056 | tf_op jit(solution)/shard_map/all_to_all | solution.py:16
  13.2 0.8 fusion.21
  13.9 0.1 broadcast_in_dim.15
  14.0 26.7 %all_to_all.62 = bf16[32,32,256]{2,1,0:T(8,128)(2,1)S(1)} all-to-all(bf16[32,32,256]{2,1,0:T(8,128)(2,1)S(1)} %broadcast_in_dim.15), channel_id=1, replica_groups=mesh['kv'=32,'tp'=8] {'kv'}, dimensions={0} | all-to-all | bytes 1048576 | tf_op jit(solution)/shard_map/all_to_all | solution.py:16
  40.7 1.2 convolution_convert_fusion.5
  41.9 1.2 convolution_convert_fusion.6
  43.1 0.0 copy-start.12
  43.1 0.0 copy-start.13
  43.2 0.0 copy-start.20
  43.2 0.0 copy-start.14
  43.3 0.0 copy-start.5
  43.3 0.1 copy_bitcast_fusion.1
  43.5 0.0 copy-start.21
  43.5 0.0 copy-start.2
  43.5 16.5 %all_to_all.63 = bf16[8,128,352]{1,2,0:T(8,128)(2,1)S(1)} all-to-all(bf16[8,128,352]{1,2,0:T(8,128)(2,1)S(1)} %copy_bitcast_fusion.1), channel_id=1, replica_groups=mesh['kv'=32,'tp'=8] {'tp'}, dimensions={0} | all-to-all | bytes 1441792 | tf_op jit(solution)/shard_map/all_to_all | solution.py:43
  59.9 0.1 convert_reduce_fusion.1
  60.1 11.2 %all_to_all.64 = bf16[8,128,176]{1,2,0:T(8,128)(2,1)S(1)} all-to-all(bf16[8,128,176]{1,2,0:T(8,128)(2,1)S(1)} %broadcast_in_dim.16), channel_id=1, replica_groups=mesh['kv'=32,'tp'=8] {'tp'}, dimensions={0} | all-to-all | bytes 720896 | tf_op jit(solution)/shard_map/all_to_all | solution.py:16
  71.4 1.1 convolution_convert_fusion.2
  72.5 4.4 %all-to-all-start.4 = ((bf16[32,32,256]{2,1,0:T(8,128)(2,1)}), bf16[32,32,256]{2,1,0:T(8,128)(2,1)S(1)}, u32[]{:S(2)}, u32[]{:S(2)}) async-start(bf16[32,32,256]{2,1,0:T(8,128)(2,1)} %bitcast.84), calls=%async_computation.4 | async-start | bytes 1048576 | tf_op jit(solution)/shard_map/all_to_all | solution.py:43
  77.1 15.3 %all-to-all-done.4 = bf16[32,32,256]{2,1,0:T(8,128)(2,1)S(1)} async-done(((bf16[32,32,256]{2,1,0:T(8,128)(2,1)}), bf16[32,32,256]{2,1,0:T(8,128)(2,1)S(1)}, u32[]{:S(2)}, u32[]{:S(2)}) %all-to-all-start.4) | async-done | bytes 524320 | tf_op jit(solution)/shard_map/all_to_all | solution.py:43
  92.4 0.1 convert_reduce_fusion.3
  92.5 0.7 broadcast_in_dim.17
  93.2 6.4 %all-to-all-start.5 = ((bf16[8,32,256]{2,1,0:T(8,128)(2,1)}), bf16[8,32,256]{2,1,0:T(8,128)(2,1)S(1)}, u32[]{:S(2)}, u32[]{:S(2)}) async-start(bf16[8,32,256]{2,1,0:T(8,128)(2,1)} %broadcast_in_dim.17), calls=%async_computation.5 | async-start | bytes 262144 | tf_op jit(solution)/shard_map/all_to_all | solution.py:16
  99.6 5.2 %all-to-all-done.5 = bf16[8,32,256]{2,1,0:T(8,128)(2,1)S(1)} async-done(((bf16[8,32,256]{2,1,0:T(8,128)(2,1)}), bf16[8,32,256]{2,1,0:T(8,128)(2,1)S(1)}, u32[]{:S(2)}, u32[]{:S(2)}) %all-to-all-start.5) | async-done | bytes 131104 | tf_op jit(solution)/shard_map/all_to_all | solution.py:16
  104.9 0.1 fusion.16
  105.1 0.1 multiply_convert_fusion
  105.2 0.2 multiply_exponential_fusion
  105.4 0.1 copy.66
  105.4 0.1 copy.67
  105.5 0.3 divide_multiply_fusion
  105.9 0.1 reshape.157
  106.0 0.1 broadcast_multiply_fusion
  106.1 0.2 divide_multiply_fusion.1
  106.3 1.3 divide_multiply_fusion.2
  107.6 3.1 %multiply_add_fusion = f32[32,4,64,128]{3,2,1,0:T(8,128)S(1)} fusion(f32[32,4,64,128]{3,2,1,0:T(8,128)} %param.47, f32[32,128]{1,0:T(8,128)S(1)} %divide_multiply_fusion.2, f32[32,4,64]{2,1,0:T(4,128)S(1)} %broadcast_multiply_fusion, f32[32,4]{1,0:T(8,128)S(1)} %copy.66), kind=kLoop, calls=%fused_computation | loop fusion | flops 3145728 | bytes 8438272 | tf_op jit(solution)/shard_map/add | solution.py:135
  110.7 2.0 copy-done.1
  112.7 1.7 fusion.30
  114.4 0.1 fusion.27
  114.5 0.1 reshape.167
  114.6 0.4 multiply_reduce_fusion.3
  115.0 0.3 convolution_convert_fusion
  115.4 8.5 %all_to_all.65 = bf16[8,32,256]{2,1,0:T(8,128)(2,1)S(1)} all-to-all(bf16[8,32,256]{2,1,0:T(8,128)(2,1)S(1)} %bitcast.86), channel_id=1, replica_groups=mesh['kv'=32,'tp'=8] {'tp'}, dimensions={0} | all-to-all | bytes 262144 | tf_op jit(solution)/shard_map/all_to_all | solution.py:43
  123.9 0.1 fusion.23
  124.0 0.6 broadcast_in_dim.18
  124.6 4.1 %all-to-all-start.7 = ((f32[8,1,32]{2,1,0:T(1,128)}), f32[8,1,32]{2,1,0:T(1,128)S(1)}, u32[]{:S(2)}, u32[]{:S(2)}) async-start(f32[8,1,32]{2,1,0:T(1,128)} %broadcast_in_dim.18), calls=%async_computation.7 | async-start | bytes 8192 | tf_op jit(solution)/shard_map/all_to_all | solution.py:16
  128.7 4.5 %all-to-all-done.7 = f32[8,1,32]{2,1,0:T(1,128)S(1)} async-done(((f32[8,1,32]{2,1,0:T(1,128)}), f32[8,1,32]{2,1,0:T(1,128)S(1)}, u32[]{:S(2)}, u32[]{:S(2)}) %all-to-all-start.7) | async-done | bytes 1056 | tf_op jit(solution)/shard_map/all_to_all | solution.py:16
  133.3 0.1 fusion.25
  133.3 0.1 broadcast_in_dim.19
  133.4 20.5 %all_to_all.66 = bf16[32,32,256]{2,1,0:T(8,128)(2,1)S(1)} all-to-all(bf16[32,32,256]{2,1,0:T(8,128)(2,1)S(1)} %broadcast_in_dim.19), channel_id=1, replica_groups=mesh['kv'=32,'tp'=8] {'kv'}, dimensions={0} | all-to-all | bytes 1048576 | tf_op jit(solution)/shard_map/all_to_all | solution.py:16
  153.9 0.3 convolution_convert_fusion.3
  154.2 0.3 convolution_convert_fusion.4
  154.6 0.1 copy_bitcast_fusion
  154.8 16.3 %all_to_all.67 = bf16[8,128,352]{1,2,0:T(8,128)(2,1)S(1)} all-to-all(bf16[8,128,352]{1,2,0:T(8,128)(2,1)S(1)} %copy_bitcast_fusion), channel_id=1, replica_groups=mesh['kv'=32,'tp'=8] {'tp'}, dimensions={0} | all-to-all | bytes 1441792 | tf_op jit(solution)/shard_map/all_to_all | solution.py:43
  171.1 0.1 convert_reduce_fusion
  171.3 11.1 %all_to_all.68 = bf16[8,128,176]{1,2,0:T(8,128)(2,1)S(1)} all-to-all(bf16[8,128,176]{1,2,0:T(8,128)(2,1)S(1)} %broadcast_in_dim.20), channel_id=1, replica_groups=mesh['kv'=32,'tp'=8] {'tp'}, dimensions={0} | all-to-all | bytes 720896 | tf_op jit(solution)/shard_map/all_to_all | solution.py:16
  182.3 0.3 convolution_convert_fusion.1
  182.7 19.7 %all_to_all.69 = bf16[32,32,256]{2,1,0:T(8,128)(2,1)S(1)} all-to-all(bf16[32,32,256]{2,1,0:T(8,128)(2,1)S(1)} %bitcast.85), channel_id=1, replica_groups=mesh['kv'=32,'tp'=8] {'kv'}, dimensions={0} | all-to-all | bytes 1048576 | tf_op jit(solution)/shard_map/all_to_all | solution.py:43
  202.5 0.1 convert_reduce_fusion.2
  202.5 0.6 fusion.26
  (69 shorter events, 0.6 us)
Async XLA Ops:
  0.6 114.4 %copy-start = (bf16[256,2048]{1,0:T(8,128)(2,1)S(1)}, bf16[256,2048]{1,0:T(8,128)(2,1)}, u32[]{:S(2)}) copy-start(bf16[256,2048]{1,0:T(8,128)(2,1)} %param.49) | copy-start | bytes 3145732
  2.2 11.0 %all-to-all-start = ((f32[8,1,32]{2,1,0:T(1,128)}), f32[8,1,32]{2,1,0:T(1,128)S(1)}, u32[]{:S(2)}, u32[]{:S(2)}) async-start(f32[8,1,32]{2,1,0:T(1,128)} %broadcast_in_dim.14), calls=%async_computation | async-start | bytes 8192 | tf_op jit(solution)/shard_map/all_to_all | solution.py:16
  40.7 30.7 %copy-start.16 = (bf16[176,256]{1,0:T(8,128)(2,1)S(1)}, bf16[176,256]{1,0:T(8,128)(2,1)}, u32[]{:S(2)}) copy-start(bf16[176,256]{1,0:T(8,128)(2,1)} %param.31) | copy-start | bytes 270340
  43.1 33.7 %copy-start.12 = (bf16[4,128]{1,0:T(4,128)(2,1)S(1)}, bf16[4,128]{1,0:T(4,128)(2,1)}, u32[]{:S(2)}) copy-start(bf16[4,128]{1,0:T(4,128)(2,1)} %param.42) | copy-start | bytes 3076
  43.1 33.8 %copy-start.13 = (bf16[4,128]{1,0:T(4,128)(2,1)S(1)}, bf16[4,128]{1,0:T(4,128)(2,1)}, u32[]{:S(2)}) copy-start(bf16[4,128]{1,0:T(4,128)(2,1)} %param.43) | copy-start | bytes 3076
  43.2 33.8 %copy-start.11 = (bf16[4,256]{1,0:T(4,128)(2,1)S(1)}, bf16[4,256]{1,0:T(4,128)(2,1)}, u32[]{:S(2)}) copy-start(bf16[4,256]{1,0:T(4,128)(2,1)} %param.41) | copy-start | bytes 6148
  43.2 33.8 %copy-start.19 = (f32[4]{0:T(128)S(1)}, f32[4]{0:T(128)}, u32[]{:S(2)}) copy-start(f32[4]{0:T(128)} %param.39) | copy-start | bytes 52
  43.2 33.8 %copy-start.20 = (bf16[256]{0:T(256)(128)(2,1)S(1)}, bf16[256]{0:T(256)(128)(2,1)}, u32[]{:S(2)}) copy-start(bf16[256]{0:T(256)(128)(2,1)} %param.48) | copy-start | bytes 1540
  43.2 33.8 %copy-start.14 = (bf16[2048]{0:T(1024)(128)(2,1)S(1)}, bf16[2048]{0:T(1024)(128)(2,1)}, u32[]{:S(2)}) copy-start(bf16[2048]{0:T(1024)(128)(2,1)} %param.32) | copy-start | bytes 12292
  43.2 33.8 %copy-start.9 = (bf16[32,3,128]{2,0,1:T(8,128)(2,1)S(1)}, bf16[32,3,128]{2,0,1:T(8,128)(2,1)}, u32[]{:S(2)}) copy-start(bf16[32,3,128]{2,0,1:T(8,128)(2,1)} %param.46) | copy-start | bytes 73732
  43.2 33.9 %copy-start.10 = (bf16[32,3,128]{2,0,1:T(8,128)(2,1)S(1)}, bf16[32,3,128]{2,0,1:T(8,128)(2,1)}, u32[]{:S(2)}) copy-start(bf16[32,3,128]{2,0,1:T(8,128)(2,1)} %param.45) | copy-start | bytes 73732
  43.3 49.2 %copy-start.5 = (bf16[32,256]{1,0:T(8,128)(2,1)S(1)}, bf16[32,256]{1,0:T(8,128)(2,1)}, u32[]{:S(2)}) copy-start(bf16[32,256]{1,0:T(8,128)(2,1)} %param.27) | copy-start | bytes 49156
  43.3 56.3 %copy-start.8 = (bf16[32,3,256]{2,0,1:T(8,128)(2,1)S(1)}, bf16[32,3,256]{2,0,1:T(8,128)(2,1)}, u32[]{:S(2)}) copy-start(bf16[32,3,256]{2,0,1:T(8,128)(2,1)} %param.44) | copy-start | bytes 147460
  43.4 61.7 %copy-start.18 = (bf16[2048,4]{0,1:T(4,128)(2,1)S(1)}, bf16[2048,4]{0,1:T(4,128)(2,1)}, u32[]{:S(2)}) copy-start(bf16[2048,4]{0,1:T(4,128)(2,1)} %param.37) | copy-start | bytes 49156
  43.5 61.7 %copy-start.21 = (f32[4]{0:T(128)S(1)}, f32[4]{0:T(128)}, u32[]{:S(2)}) copy-start(f32[4]{0:T(128)} %param.38) | copy-start | bytes 52
  43.5 62.1 %copy-start.2 = (bf16[2048,256]{1,0:T(8,128)(2,1)S(1)}, bf16[2048,256]{1,0:T(8,128)(2,1)}, u32[]{:S(2)}) copy-start(bf16[2048,256]{1,0:T(8,128)(2,1)} %param.34) | copy-start | bytes 3145732
  60.0 46.0 %copy-start.4 = (bf16[2048,128]{1,0:T(8,128)(2,1)S(1)}, bf16[2048,128]{1,0:T(8,128)(2,1)}, u32[]{:S(2)}) copy-start(bf16[2048,128]{1,0:T(8,128)(2,1)} %param.36) | copy-start | bytes 1572868
  72.5 19.9 %all-to-all-start.4 = ((bf16[32,32,256]{2,1,0:T(8,128)(2,1)}), bf16[32,32,256]{2,1,0:T(8,128)(2,1)S(1)}, u32[]{:S(2)}, u32[]{:S(2)}) async-start(bf16[32,32,256]{2,1,0:T(8,128)(2,1)} %bitcast.84), calls=%async_computation.4 | async-start | bytes 1048576 | tf_op jit(solution)/shard_map/all_to_all | solution.py:43
  93.2 11.6 %all-to-all-start.5 = ((bf16[8,32,256]{2,1,0:T(8,128)(2,1)}), bf16[8,32,256]{2,1,0:T(8,128)(2,1)S(1)}, u32[]{:S(2)}, u32[]{:S(2)}) async-start(bf16[8,32,256]{2,1,0:T(8,128)(2,1)} %broadcast_in_dim.17), calls=%async_computation.5 | async-start | bytes 262144 | tf_op jit(solution)/shard_map/all_to_all | solution.py:16
  110.6 2.0 copy-start.1
  110.7 3.7 %copy-start.15 = (f32[4]{0:T(128)S(1)}, f32[4]{0:T(128)}, u32[]{:S(2)}) copy-start(f32[4]{0:T(128)} %param.40) | copy-start | bytes 52
  110.7 3.9 %copy-start.3 = (bf16[2048,256]{1,0:T(8,128)(2,1)S(1)}, bf16[2048,256]{1,0:T(8,128)(2,1)}, u32[]{:S(2)}) copy-start(bf16[2048,256]{1,0:T(8,128)(2,1)} %param.33) | copy-start | bytes 3145732
  110.7 18.0 %copy-start.22 = (bf16[256]{0:T(256)(128)(2,1)S(1)}, bf16[256]{0:T(256)(128)(2,1)}, u32[]{:S(2)}) copy-start(bf16[256]{0:T(256)(128)(2,1)} %param.50) | copy-start | bytes 1540
  112.7 41.2 %copy-start.6 = (bf16[256,176]{0,1:T(8,128)(2,1)S(1)}, bf16[256,176]{0,1:T(8,128)(2,1)}, u32[]{:S(2)}) copy-start(bf16[256,176]{0,1:T(8,128)(2,1)} %param.52) | copy-start | bytes 270340
  112.7 41.6 %copy-start.7 = (bf16[256,176]{0,1:T(8,128)(2,1)S(1)}, bf16[256,176]{0,1:T(8,128)(2,1)}, u32[]{:S(2)}) copy-start(bf16[256,176]{0,1:T(8,128)(2,1)} %param.51) | copy-start | bytes 270340
  124.6 8.6 %all-to-all-start.7 = ((f32[8,1,32]{2,1,0:T(1,128)}), f32[8,1,32]{2,1,0:T(1,128)S(1)}, u32[]{:S(2)}, u32[]{:S(2)}) async-start(f32[8,1,32]{2,1,0:T(1,128)} %broadcast_in_dim.18), calls=%async_computation.7 | async-start | bytes 8192 | tf_op jit(solution)/shard_map/all_to_all | solution.py:16
  153.9 28.5 %copy-start.17 = (bf16[176,256]{1,0:T(8,128)(2,1)S(1)}, bf16[176,256]{1,0:T(8,128)(2,1)}, u32[]{:S(2)}) copy-start(bf16[176,256]{1,0:T(8,128)(2,1)} %param.53) | copy-start | bytes 270340
where the time goes:
time: 205 us; the launch traced here: 203 us
  blocking collectives  130 us (63%)
  waiting for transfers between devices  29 us (14%)
  starting transfers between devices  21.2 us (10%)
  matrix products  8.98 us (4%)
  other arithmetic  7.38 us (4%)
  local copies, waits for them, and re-layouts  4.87 us (2%)
    all_to_all x4, blocking collectives, sent_to_all(): lax.all_to_all(jnp.broadcast_to(array[None], (length, *array.shape)), axi...  69.4 us
    all_to_all x4, blocking collectives, sum_at_owner(): lax.all_to_all(in_blocks(array, dim, length), axis, 0, 0, tiled=True)  61 us
    all_to_all x3, starting transfers between devices, sent_to_all(): lax.all_to_all(jnp.broadcast_to(array[None], (length, *array.shape)), axi...  16.9 us
    all_to_all x1, waiting for transfers between devices, sum_at_owner(): lax.all_to_all(in_blocks(array, dim, length), axis, 0, 0, tiled=True)  15.3 us
    all_to_all x3, waiting for transfers between devices, sent_to_all(): lax.all_to_all(jnp.broadcast_to(array[None], (length, *array.shape)), axi...  13.7 us
    all_to_all x1, starting transfers between devices, sum_at_owner(): lax.all_to_all(in_blocks(array, dim, length), axis, 0, 0, tiled=True)  4.37 us
  transfers between devices with their start and end apart: 4, of which 4 were waited for; matrix products, arithmetic and copies ran while one was open for 0% of the time, Pallas kernels for 0%

commit v1 on v0

v1 whole, which is shorter than its diff:
```python
import jax
import jax.numpy as jnp
from jax import lax
from jax.experimental import pallas as pl
from jax.experimental.pallas import tpu as pltpu
from jax.sharding import PartitionSpec as P

D = 2048
HEAD_DIM = 64
STATE = 128
EPS = 1e-06

NZ, NY, NT = 8, 4, 8
NKV = NZ * NY
RPT = 4
QW = 512
SEQ = 32
GROUP = 256
Z_ORDER_NEAR = (1, 7, 2, 6, 3, 5, 4)
Z_ORDER_FAR = (4, 3, 5, 2, 6, 1, 7, 0)
MESH = pl.DeviceIdType.MESH
F32, BF16 = jnp.float32, jnp.bfloat16


def dot(a, b):
    return jnp.dot(a, b, preferred_element_type=F32)


def iota2(shape, dim):
    return lax.broadcasted_iota(jnp.int32, shape, dim)


def gather_rows(n):
    shape = (16 * n, 16 * n)
    row, col = iota2(shape, 0), iota2(shape, 1)
    q, rest = row // (4 * n), row % (4 * n)
    return (col == (rest // 4) * 16 + q * 4 + rest % 4).astype(BF16)


def scatter_rows(n):
    shape = (16 * n, 16 * n)
    row, col = iota2(shape, 0), iota2(shape, 1)
    q, rest = col // (4 * n), col % (4 * n)
    return (row == (rest // 4) * 16 + q * 4 + rest % 4).astype(BF16)


def piece_factor(piece):
    partial = jnp.sum(piece * piece, axis=1, keepdims=True)
    same = (iota2((16, 16), 0) % 4 == iota2((16, 16), 1) % 4).astype(F32)
    total = jnp.dot(
        same,
        jnp.broadcast_to(partial, (16, 128)),
        preferred_element_type=F32,
        precision=lax.Precision.HIGHEST,
    )
    return lax.rsqrt(total[:, :1] / D + EPS)


def kernel(
    msg_ref, mgain_ref, par_ref, conv_ref,
    fg_ref, fl_ref, fd_ref, sg_ref, sl_ref, sd_ref,
    pg_ref, pi_ref, pw_ref, pr_ref, ps_ref, po_ref, scan_ref,
    out_ref, retain_ref, u_ref, bc_ref,
    recv_r, wg1, wl1, wd1, wg2, wl2, wd2,
    ag1, ag2, perm, permt, hid, psend, ry1, zs1, rz1, ry2, zs2, rz2,
    send_f, recv_f, recv_o, send_o, send_q, recv_q,
    pgv, piv, pwv, prv, psv, pov, scan_f, scan_b, xrow, gsplit,
    loc_sem, s_r, r_r, s_w, r_w, s_ag, r_ag, s_y, r_y, s_z, r_z, s_f, r_f, s_o, r_o, s_q, r_q,
):
    kv = lax.axis_index("kv")
    t = lax.axis_index("tp")
    z, y = kv // NY, kv % NY
    core = t % 2

    def zpeer(d):
        return lax.rem(z + d, NZ)

    def ypeer(d):
        return lax.rem(y + d, NY)

    def tpeer(d):
        return lax.rem(t + d, NT)

    def rcopy(src, dst, ssem, rsem, dev):
        return pltpu.make_async_remote_copy(
            src_ref=src, dst_ref=dst, send_sem=ssem, recv_sem=rsem, device_id=dev, device_id_type=MESH
        )

    locals_ = []

    def local(src, dst, k):
        copy = pltpu.make_async_copy(src, dst, loc_sem.at[k])
        copy.start()
        return copy

    l_msg = local(msg_ref.at[t], recv_r.at[t], 0)
    l_w1 = [local(fg_ref, wg1.at[t], 1), local(fl_ref, wl1.at[t], 2), local(fd_ref, wd1.at[t], 3)]

    barrier = pltpu.get_barrier_semaphore()
    peers = [(zpeer(d) * NY + y, t) for d in range(1, NZ)]
    peers += [(z * NY + ypeer(d), t) for d in range(1, NY)]
    peers += [(kv, tpeer(d)) for d in range(1, NT)]
    for dev in peers:
        pl.semaphore_signal(barrier, inc=1, device_id=dev, device_id_type=MESH)

    perm[...] = gather_rows(NKV)
    permt[...] = scatter_rows(NKV)
    pl.semaphore_wait(barrier, len(peers))

    sends_r = []
    for d in range(1, NT):
        tt = tpeer(d)
        c = rcopy(msg_ref.at[tt], recv_r.at[t], s_r.at[d], r_r.at[d], (kv, tt))
        c.start()
        sends_r.append(c)

    def start_weights(k, src, dst):
        copies = []
        for j in range(1, 4):
            tt = lax.rem(t + 2 * j, NT)
            c = rcopy(src, dst.at[t], s_w.at[k, j], r_w.at[k, j], (kv, tt))
            c.start()
            copies.append(c)
        c = rcopy(src, dst.at[t], s_w.at[k, 0], r_w.at[k, 0], (kv, t + 1 - 2 * core))
        c.start()
        copies.append(c)
        return copies

    def forward_weights(k, dst):
        copies = []
        for j in range(1, 4):
            ss = lax.rem(t - 2 * j + NT, NT)
            rcopy(dst.at[ss], dst.at[ss], s_w.at[k, j], r_w.at[k, j], (kv, ss)).wait_recv()
            c = rcopy(dst.at[ss], dst.at[ss], s_w.at[k, 3 + j], r_w.at[k, 3 + j], (kv, t + 1 - 2 * core))
            c.start()
            copies.append(c)
        return copies

    def finish_weights(k, dst, copies):
        partner = t + 1 - 2 * core
        rcopy(dst.at[partner], dst.at[partner], s_w.at[k, 0], r_w.at[k, 0], (kv, partner)).wait_recv()
        for j in range(1, 4):
            ss = lax.rem(partner - 2 * j + NT, NT)
            rcopy(dst.at[ss], dst.at[ss], s_w.at[k, 3 + j], r_w.at[k, 3 + j], (kv, partner)).wait_recv()
        for c in copies:
            c.wait_send()

    w1 = [start_weights(0, fg_ref, wg1), start_weights(1, fl_ref, wl1), start_weights(2, fd_ref, wd1)]

    l_mix = [
        local(pg_ref, pgv, 4), local(pi_ref, piv, 5), local(pw_ref, pwv, 6), local(pr_ref, prv, 7),
        local(ps_ref, psv, 8), local(po_ref, pov, 9), local(scan_ref, scan_f, 10),
    ]
    l_w2 = [local(sg_ref, wg2.at[t], 11), local(sl_ref, wl2.at[t], 12), local(sd_ref, wd2.at[t], 13)]

    l_msg.wait()
    for d in range(1, NT):
        src = lax.rem(t - d + NT, NT)
        rcopy(recv_r.at[src], recv_r.at[src], s_r.at[d], r_r.at[d], (kv, src)).wait_recv()

    row, col = iota2((48, 64), 0), iota2((48, 64), 1)
    pick = (col == ((row % 16) // 4) * 16 + (row // 16) * 4 + row % 4).astype(BF16)
    halves = []
    for h in range(2):
        block = jnp.concatenate([recv_r[2 * q + h] for q in range(4)], axis=0)
        halves.append(dot(pick, block))
    both = jnp.concatenate(halves, axis=1)
    res1 = both[0:16]
    gsplit[...] = both[16:48]

    def start_gather(ag, f):
        me = kv
        copies = []
        for d in (4, 3, 5, 2, 6, 1, 7):
            c = rcopy(ag.at[me], ag.at[me], s_ag.at[f, 0, d], r_ag.at[f, 0, d], (zpeer(d) * NY + y, t))
            c.start()
            copies.append(c)
        for e in (2, 1, 3):
            c = rcopy(ag.at[me], ag.at[me], s_ag.at[f, e, 0], r_ag.at[f, e, 0], (z * NY + ypeer(e), t))
            c.start()
            copies.append(c)
        return copies

    def forward_gather(ag, f, copies):
        for d in Z_ORDER_NEAR:
            slot = lax.rem(z - d + NZ, NZ) * NY + y
            rcopy(ag.at[slot], ag.at[slot], s_ag.at[f, 0, d], r_ag.at[f, 0, d], (slot, t)).wait_recv()
            for e in (2, 1, 3):
                c = rcopy(ag.at[slot], ag.at[slot], s_ag.at[f, e, d], r_ag.at[f, e, d], (z * NY + ypeer(e), t))
                c.start()
                copies.append(c)

    def finish_gather(ag, f, copies):
        for d in (0,) + Z_ORDER_NEAR:
            for e in (1, 3, 2):
                slot = lax.rem(z - d + NZ, NZ) * NY + lax.rem(y - e + NY, NY)
                src = z * NY + lax.rem(y - e + NY, NY)
                rcopy(ag.at[slot], ag.at[slot], s_ag.at[f, e, d], r_ag.at[f, e, d], (src, t)).wait_recv()
        for c in copies:
            c.wait_send()

    def feed_forward(ag, wg, wl, wd):
        flat = ag[...].reshape(16 * NKV, QW)
        lhs = dot(perm[...], flat).astype(BF16)
        gate, lift = None, None
        for s in range(NT):
            q, h = s // 2, s % 2
            part = lhs[128 * q : 128 * q + 128, 256 * h : 256 * h + 256]
            g, u = dot(part, wg[s]), dot(part, wl[s])
            gate = g if gate is None else gate + g
            lift = u if lift is None else lift + u
        hidden = (gate * jax.nn.sigmoid(gate) * lift).astype(BF16)
        for s in range(NT):
            q, h = s // 2, s % 2
            hid[128 * q : 128 * q + 128, 256 * h : 256 * h + 256] = dot(hidden, wd[s]).astype(BF16)
        psend[...] = dot(permt[...], hid[...]).astype(BF16).reshape(NKV, 16, QW)

    def reduce_start(ry, f):
        copies = []
        for d in Z_ORDER_FAR:
            zz = zpeer(d)
            for e in (2, 1, 3):
                yy = ypeer(e)
                c = rcopy(psend.at[zz * NY + yy], ry.at[e, d], s_y.at[f, e, d], r_y.at[f, e, d], (z * NY + yy, t))
                c.start()
                copies.append(c)
        return copies

    def reduce_finish(ry, zs, rz, f, copies):
        own = None
        for d in Z_ORDER_FAR:
            zz = zpeer(d)
            total = psend[zz * NY + y].astype(F32)
            for e in (1, 3, 2):
                src = z * NY + lax.rem(y - e + NY, NY)
                rcopy(psend.at[0], ry.at[e, d], s_y.at[f, e, d], r_y.at[f, e, d], (src, t)).wait_recv()
                total = total + ry[e, d].astype(F32)
            if d == 0:
                own = total
            else:
                zs[d] = total.astype(BF16)
                c = rcopy(zs.at[d], rz.at[d], s_z.at[f, d], r_z.at[f, d], (zz * NY + y, t))
                c.start()
                copies.append(c)
        for d in range(1, NZ):
            src = lax.rem(z - d + NZ, NZ) * NY + y
            rcopy(zs.at[d], rz.at[d], s_z.at[f, d], r_z.at[f, d], (src, t)).wait_recv()
            own = own + rz[d].astype(F32)
        for c in copies:
            c.wait_send()
        return own

    ag1[kv] = (res1 * piece_factor(res1) * gsplit[0:16]).astype(BF16)
    a_copies = start_gather(ag1, 0)
    forward_gather(ag1, 0, a_copies)
    for k, dst in enumerate((wg1, wl1, wd1)):
        w1[k] += forward_weights(k, dst)
    finish_gather(ag1, 0, a_copies)
    for copy in l_w1:
        copy.wait()
    for k, dst in enumerate((wg1, wl1, wd1)):
        finish_weights(k, dst, w1[k])
    feed_forward(ag1, wg1, wl1, wd1)
    y_copies = reduce_start(ry1, 0)
    w2 = [start_weights(3, sg_ref, wg2), start_weights(4, sl_ref, wl2)]
    for copy in l_mix:
        copy.wait()
    scan_b[...] = scan_f[...].astype(BF16)
    branch = reduce_finish(ry1, zs1, rz1, 0, y_copies)
    first = (res1 + 0.5 * branch).astype(BF16).astype(F32)

    send_f[...] = (first * piece_factor(first) * mgain_ref[...]).astype(BF16)
    f_copies = []
    for d in range(1, NT):
        c = rcopy(send_f, recv_f.at[d], s_f.at[d], r_f.at[d], (kv, tpeer(d)))
        c.start()
        f_copies.append(c)
    recv_f[0] = send_f[...]
    row, col = iota2((128, 128), 0), iota2((128, 128), 1)
    q_, i_, r_ = row // 32, (row % 32) // 4, row % 4
    slot_ = lax.rem(t - i_ + NT, NT)
    perm8 = (col == slot_ * 16 + q_ * 4 + r_).astype(BF16)
    for d in range(1, NT):
        src = lax.rem(t - d + NT, NT)
        rcopy(send_f, recv_f.at[d], s_f.at[d], r_f.at[d], (kv, src)).wait_recv()
    rows = dot(perm8, recv_f[...].reshape(128, QW)).astype(BF16)
    for q in range(4):
        xrow[:, QW * q : QW * q + QW] = rows[32 * q : 32 * q + 32]
    mixed_in = xrow[...]

    def project(w):
        return dot(mixed_in, w[...]).astype(BF16).astype(F32)

    gate_z, input_new = project(pgv), project(piv)
    write_new, read_new, step_raw4 = project(pwv), project(prv), project(psv)

    def silu(v):
        return v * jax.nn.sigmoid(v)

    xc = silu(conv_ref[:, 0:256] + input_new * par_ref[4:5, :])
    bc = silu(conv_ref[:, 256:384] + write_new * par_ref[5:6, 0:128])
    rc = silu(conv_ref[:, 384:512] + read_new * par_ref[5:6, 128:256])
    lane_head = iota2((SEQ, GROUP), 1) // HEAD_DIM
    step_raw = jnp.zeros((SEQ, GROUP), F32)
    for h in range(4):
        step_raw = jnp.where(lane_head == h, step_raw4[:, h : h + 1], step_raw)
    pre = step_raw + par_ref[0:1, :]
    step = jnp.maximum(pre, 0.0) + jnp.log1p(jnp.exp(-jnp.abs(pre)))
    retain = jnp.exp(-step * jnp.exp(par_ref[1:2, :]))
    u = step * xc
    retain_ref[...] = retain
    u_ref[...] = u
    bc_ref[...] = bc
    rcb = rc.astype(BF16)
    sub = iota2((8, GROUP), 0)
    reads = []
    for g in range(4):
        acc = jnp.zeros((8, GROUP), F32)
        for j in range(8):
            b = 8 * g + j
            got = lax.dot_general(
                rcb[8 * g : 8 * g + 8], scan_b[b], (((1,), (1,)), ((), ())), preferred_element_type=F32
            )
            acc = jnp.where(sub == j, got, acc)
        reads.append(acc)
    read = jnp.concatenate(reads, axis=0)
    head = retain * read + u * jnp.sum(bc * rc, axis=1, keepdims=True) + par_ref[2:3, :] * xc
    gated = head.astype(BF16).astype(F32) * silu(gate_z)
    gated = gated * lax.rsqrt(jnp.mean(gated * gated, axis=1, keepdims=True) + EPS) * par_ref[3:4, :]
    part = dot(gated.astype(BF16), pov[...]).astype(BF16)
    stacked = jnp.concatenate([part[:, QW * q : QW * q + QW] for q in range(4)], axis=0)
    send_o[...] = dot(scatter_rows(NT), stacked).astype(BF16).reshape(NT, 16, QW)
    o_copies = []
    for d in range(1, NT):
        tt = tpeer(d)
        c = rcopy(send_o.at[tt], recv_o.at[d], s_o.at[d], r_o.at[d], (kv, tt))
        c.start()
        o_copies.append(c)
    for copy in l_w2:
        copy.wait()
    w2.append(start_weights(5, sd_ref, wd2))
    mixed = first + send_o[t].astype(F32)
    for d in range(1, NT):
        src = lax.rem(t - d + NT, NT)
        rcopy(send_f, recv_o.at[d], s_o.at[d], r_o.at[d], (kv, src)).wait_recv()
        mixed = mixed + recv_o[d].astype(F32)
    res2 = mixed.astype(BF16).astype(F32)

    ag2[kv] = (res2 * piece_factor(res2) * gsplit[16:32]).astype(BF16)
    a_copies = start_gather(ag2, 1)
    w2[0] += forward_weights(3, wg2)
    w2[1] += forward_weights(4, wl2)
    forward_gather(ag2, 1, a_copies)
    w2[2] += forward_weights(5, wd2)
    finish_gather(ag2, 1, a_copies)
    for k, dst in enumerate((wg2, wl2, wd2)):
        finish_weights(3 + k, dst, w2[k])
    feed_forward(ag2, wg2, wl2, wd2)
    y_copies = reduce_start(ry2, 1)
    branch = reduce_finish(ry2, zs2, rz2, 1, y_copies)
    final = (res2 + 0.5 * branch).astype(BF16)

    row, col = iota2((64, 16), 0), iota2((64, 16), 1)
    spread = ((col == (row // 16) * 4 + row % 16) & (row % 16 < 4)).astype(BF16)
    for h in range(2):
        block = dot(spread, final[:, 256 * h : 256 * h + 256]).astype(BF16).reshape(4, 16, 256)
        for q in range(4):
            send_q[2 * q + h] = block[q]
    q_copies = []
    for d in range(1, NT):
        tt = tpeer(d)
        c = rcopy(send_q.at[tt], recv_q.at[d], s_q.at[d], r_q.at[d], (kv, tt))
        c.start()
        q_copies.append(c)
    recv_q[0] = send_q[t]
    for d in range(1, NT):
        src = lax.rem(t - d + NT, NT)
        rcopy(send_q.at[0], recv_q.at[d], s_q.at[d], r_q.at[d], (kv, src)).wait_recv()
    row, col = iota2((32, 128), 0), iota2((32, 128), 1)
    pick32 = (col == lax.rem(t - row // 4 + NT, NT) * 16 + row % 4).astype(BF16)
    out_ref[...] = dot(pick32, recv_q[...].reshape(128, 256)).astype(BF16)

    for c in sends_r + f_copies + o_copies + q_copies:
        c.wait_send()


def per_device(
    residual, first_gain, first_gate, first_lift, first_down, mixer_gain,
    proj_gate, proj_input, proj_write, proj_read, proj_step,
    step_bias, rate_log, skip_gain, taps_input, taps_write, taps_read,
    buffer_input, buffer_write, buffer_read, scan_state, group_gain, proj_output,
    second_gain, second_gate, second_lift, second_down,
):
    msg = jnp.concatenate(
        [
            residual.reshape(NT, RPT, GROUP),
            jnp.broadcast_to(first_gain[None, None, :], (NT, RPT, GROUP)),
            jnp.broadcast_to(second_gain[None, None, :], (NT, RPT, GROUP)),
            jnp.zeros((NT, RPT, GROUP), BF16),
        ],
        axis=1,
    )
    mgain = jnp.repeat(mixer_gain.astype(F32).reshape(4, QW), RPT, axis=0)
    taps = jnp.concatenate([taps_input, taps_write, taps_read], axis=1).astype(F32)
    conv = jnp.concatenate(
        [
            jnp.sum(buf.astype(F32) * tap[None, :3, :].astype(F32), axis=1)
            for buf, tap in ((buffer_input, taps_input), (buffer_write, taps_write), (buffer_read, taps_read))
        ],
        axis=1,
    )
    par = jnp.stack(
        [
            jnp.repeat(step_bias, HEAD_DIM), jnp.repeat(rate_log, HEAD_DIM), jnp.repeat(skip_gain, HEAD_DIM),
            group_gain.astype(F32), taps[3, :256], taps[3, 256:], taps[3, :256], taps[3, 256:],
        ]
    )
    scan = scan_state.reshape(SEQ, GROUP, STATE)
    vm = pl.BlockSpec(memory_space=pltpu.VMEM)
    anym = pl.BlockSpec(memory_space=pl.ANY)
    hid_cols = first_gate.shape[1]
    dma = pltpu.SemaphoreType.DMA
    out, retain, u, bc = pl.pallas_call(
        kernel,
        out_shape=(
            jax.ShapeDtypeStruct((SEQ, GROUP), BF16),
            jax.ShapeDtypeStruct((SEQ, GROUP), F32),
            jax.ShapeDtypeStruct((SEQ, GROUP), F32),
            jax.ShapeDtypeStruct((SEQ, STATE), F32),
        ),
        in_specs=[vm] * 4 + [anym] * 13,
        out_specs=(vm,) * 4,
        scratch_shapes=[
            pltpu.VMEM((NT, 16, GROUP), BF16),
            *[pltpu.VMEM((NT, 256, hid_cols), BF16), pltpu.VMEM((NT, 256, hid_cols), BF16), pltpu.VMEM((NT, hid_cols, 256), BF16)] * 2,
            pltpu.VMEM((NKV, 16, QW), BF16),
            pltpu.VMEM((NKV, 16, QW), BF16),
            pltpu.VMEM((16 * NKV, 16 * NKV), BF16),
            pltpu.VMEM((16 * NKV, 16 * NKV), BF16),
            pltpu.VMEM((512, QW), BF16),
            pltpu.VMEM((NKV, 16, QW), BF16),
            *[pltpu.VMEM((NY, NZ, 16, QW), BF16), pltpu.VMEM((NZ, 16, QW), BF16), pltpu.VMEM((NZ, 16, QW), BF16)] * 2,
            pltpu.VMEM((16, QW), BF16),
            pltpu.VMEM((NT, 16, QW), BF16),
            pltpu.VMEM((NT, 16, QW), BF16),
            pltpu.VMEM((NT, 16, QW), BF16),
            pltpu.VMEM((NT, 16, GROUP), BF16),
            pltpu.VMEM((NT, 16, GROUP), BF16),
            pltpu.VMEM((D, 256), BF16),
            pltpu.VMEM((D, 256), BF16),
            pltpu.VMEM((D, 128), BF16),
            pltpu.VMEM((D, 128), BF16),
            pltpu.VMEM((D, 4), BF16),
            pltpu.VMEM((256, D), BF16),
            pltpu.VMEM((SEQ, GROUP, STATE), F32),
            pltpu.VMEM((SEQ, GROUP, STATE), BF16),
            pltpu.VMEM((SEQ, D), BF16),
            pltpu.VMEM((32, QW), F32),
            dma((14,)),
            dma((NT,)), dma((NT,)),
            dma((6, 7)), dma((6, 7)),
            dma((2, NY, NZ)), dma((2, NY, NZ)),
            dma((2, NY, NZ)), dma((2, NY, NZ)),
            dma((2, NZ)), dma((2, NZ)),
            dma((NT,)), dma((NT,)),
            dma((NT,)), dma((NT,)),
            dma((NT,)), dma((NT,)),
        ],
        compiler_params=pltpu.CompilerParams(
            collective_id=0, has_side_effects=True, vmem_limit_bytes=56 * 1024 * 1024
        ),
        name="layer",
    )(
        msg, mgain, par, conv,
        first_gate, first_lift, first_down, second_gate, second_lift, second_down,
        proj_gate, proj_input, proj_write, proj_read, proj_step, proj_output, scan,
    )
    heads = scan_state.shape[1]
    state_out = (
        retain[:, ::HEAD_DIM][:, :, None, None] * scan_state
        + u.reshape(SEQ, heads, HEAD_DIM)[..., None] * bc[:, None, None, :]
    )
    return out, state_out


def solution(mesh):
    placed = (
        P("kv", "tp"), P("tp"), P("tp", "kv"), P("tp", "kv"), P("kv", "tp"), P(),
        P(None, "tp"), P(None, "tp"), P(None, "tp"), P(None, "tp"), P(None, "tp"),
        P("tp"), P("tp"), P("tp"), P(None, "tp"), P(None, "tp"), P(None, "tp"),
        P("kv", None, "tp"), P("kv", None, "tp"), P("kv", None, "tp"), P("kv", "tp", None, None),
        P("tp"), P("tp", None), P("tp"), P("tp", "kv"), P("tp", "kv"), P("kv", "tp"),
    )
    return jax.shard_map(
        per_device,
        mesh=mesh,
        in_specs=placed,
        out_specs=(P("kv", "tp"), P("kv", "tp", None, None)),
        check_vma=False,
    )
```

time: 205 us -> 118 us (0.58)
  blocking collectives: 130 us -> 0 us
  Pallas kernels: 0 us -> 87 us
  waiting for transfers between devices: 29 us -> 0 us
  starting transfers between devices: 21.2 us -> 0 us
  local copies, waits for them, and re-layouts: 4.87 us -> 17.1 us
  matrix products: 8.98 us -> 0 us
  other arithmetic: 7.38 us -> 12.2 us
    all_to_all x8 -> x0, blocking collectives: 130 us -> none  [the longest x4 69.4 us: sent_to_all(): lax.all_to_all(jnp.broadcast_to(array[None], (length, *array.shape)), axi...]
    pallas_call x0 -> x1, Pallas kernels: none -> 87 us  [per_device(): pl.pallas_call(kernel, out_shape=(jax.ShapeDtypeStruct((SEQ, GROUP), BF16...]
    all_to_all x4 -> x0, waiting for transfers between devices: 29 us -> none  [the longest x1 15.3 us: sum_at_owner(): lax.all_to_all(in_blocks(array, dim, length), axis, 0, 0, tiled=True)]
    all_to_all x4 -> x0, starting transfers between devices: 21.2 us -> none  [the longest x3 16.9 us: sent_to_all(): lax.all_to_all(jnp.broadcast_to(array[None], (length, *array.shape)), axi...]
    dot_general x13 -> x0, matrix products: 8.98 us -> none  [the longest x5 2.37 us: state_project(): jnp.dot(normed, weight, preferred_element_type=jnp.float32)]
    unnamed x46 -> x8, local copies, waits for them, and re-layouts: 2.1 us -> 8.95 us
    add x1, other arithmetic: 3.08 us -> 5.82 us  [per_device(): retain[:, ::HEAD_DIM][:, :, None, None] * scan_state]
  transfers between devices with their start and end apart: 4 -> 0, of which waited for: 4 -> 0; matrix products, arithmetic and copies ran while one was open for 0% -> 0% of each run, Pallas kernels for 0% -> 0%
where the time goes in v1:
time: 118 us; the launch traced here: 117 us
  Pallas kernels  87 us (74%)
  local copies, waits for them, and re-layouts  17.1 us (14%)
  other arithmetic  12.2 us (10%)
    pallas_call x1, Pallas kernels, per_device(): pl.pallas_call(kernel, out_shape=(jax.ShapeDtypeStruct((SEQ, GROUP), BF16...  87 us
    unnamed x8, local copies, waits for them, and re-layouts  8.95 us
    add x1, other arithmetic, per_device(): retain[:, ::HEAD_DIM][:, :, None, None] * scan_state  5.82 us

profile of v1, /device:TPU:1, one launch (start us, length us, event | category | flops | bytes accessed | tf_op | source)
XLA Modules:
  0.0 117.1 jit_solution(9701115727387761938)
XLA Ops:
  0.6 0.1 pad.9.clone
  0.7 0.7 stack.12
  1.4 0.7 broadcast_in_dim.36
  2.1 0.1 stack_reshape.9
  2.2 0.7 broadcast_in_dim.37
  2.9 0.1 stack_reshape.10
  3.0 0.7 broadcast_in_dim.38
  3.7 0.1 stack_reshape.11
  3.8 0.7 slice_convert_fusion.2
  4.5 0.7 slice_convert_fusion.1
  5.2 0.8 fusion
  5.9 0.6 stack.11.par_ref
  6.5 0.7 slice_convert_fusion
  7.2 0.7 reshape.36
  7.9 0.7 reshape.30
  8.7 0.7 broadcast_in_dim.14
  9.3 0.7 broadcast_in_dim.15
  10.0 0.7 maximum_maximum_fusion.msg_ref
  10.7 0.6 reshape.33.mgain_ref
  11.3 0.8 multiply_reduce_fusion
  12.1 0.8 multiply_reduce_fusion.1
  12.9 0.6 pad_maximum_fusion.conv_ref
  13.5 1.6 %copy.29.fg_ref = bf16[256,176]{1,0:T(8,128)(2,1)} copy(bf16[256,176]{0,1:T(8,128)(2,1)} %param.29) | data formatting | bytes 180224 | tf_op args[2]
  15.2 1.6 %copy.30.fl_ref = bf16[256,176]{1,0:T(8,128)(2,1)} copy(bf16[256,176]{0,1:T(8,128)(2,1)} %param.30) | data formatting | bytes 180224 | tf_op args[3]
  16.8 1.7 %copy.31.sg_ref = bf16[256,176]{1,0:T(8,128)(2,1)} copy(bf16[256,176]{0,1:T(8,128)(2,1)} %param.51) | data formatting | bytes 180224 | tf_op args[24]
  18.5 1.6 %copy.32.sl_ref = bf16[256,176]{1,0:T(8,128)(2,1)} copy(bf16[256,176]{0,1:T(8,128)(2,1)} %param.52) | data formatting | bytes 180224 | tf_op args[25]
  20.1 1.8 %copy.33.ps_ref = bf16[2048,4]{1,0:T(8,128)(2,1)} copy(bf16[2048,4]{0,1:T(4,128)(2,1)} %param.37) | data formatting | bytes 32768 | tf_op args[10]
  21.9 87.0 %layer.1 = (bf16[32,256]{1,0:T(8,128)(2,1)}, f32[32,256]{1,0:T(8,128)}, f32[32,256]{1,0:T(8,128)}, f32[32,128]{1,0:T(8,128)}) custom-call(bf16[8,16,256]{2,1,0:T(8,128)(2,1)} %maximum_maximum_fusion.msg_ref, f32[16,512]{1,0:T(8,128)} %reshape.33.mgain_ref, f32[8,256]{1,0:T(8,128)} %stack.11.par_ref, f32[32,512]{1,0:T(8,128)} %pad_maximum_fusion.conv_ref, ...), custom_call_target="tpu_custom_call" | custom-call | tf_op jit(solution)/shard_map/layer/pallas_call | solution.py:423
  108.9 0.8 slice.25
  109.8 0.9 mul.55
  110.6 0.0 copy-start
  110.6 5.8 %multiply_add_fusion = f32[32,4,64,128]{3,2,1,0:T(8,128)} fusion(f32[32,4,64,128]{3,2,1,0:T(8,128)} %param.47, f32[32,128]{1,0:T(8,128)} %get-tuple-element.9, f32[32,4,64]{2,1,0:T(4,128)S(1)} %mul.55, f32[32,4]{1,0:T(8,128)S(1)} %slice.25), kind=kLoop, calls=%fused_computation | loop fusion | flops 3145728 | bytes 8438272 | tf_op jit(solution)/shard_map/add | solution.py:480
  116.4 0.0 copy-done
  116.4 0.6 copy.35
  (2 shorter events, 0.0 us)
Async XLA Ops:
  110.6 5.8 %copy-start = (bf16[32,256]{1,0:T(8,128)(2,1)S(1)}, bf16[32,256]{1,0:T(8,128)(2,1)}, u32[]{:S(2)}) copy-start(bf16[32,256]{1,0:T(8,128)(2,1)} %get-tuple-element.16) | copy-start | bytes 49156

commit v2 on v1

v2 whole, which is shorter than its diff:
```python
import jax
import jax.numpy as jnp
from jax import lax
from jax.experimental import pallas as pl
from jax.experimental.pallas import tpu as pltpu
from jax.sharding import PartitionSpec as P

D = 2048
HEAD_DIM = 64
STATE = 128
EPS = 1e-06

NZ, NY, NT = 8, 4, 8
NKV = NZ * NY
RPT = 4
QW = 512
SEQ = 32
GROUP = 256
MESH = pl.DeviceIdType.MESH
F32, BF16 = jnp.float32, jnp.bfloat16


def dot(a, b):
    return jnp.dot(a, b, preferred_element_type=F32)


def dot_nt(a, b):
    return lax.dot_general(a, b, (((1,), (1,)), ((), ())), preferred_element_type=F32)


def iota2(shape, dim):
    return lax.broadcasted_iota(jnp.int32, shape, dim)


def gather_rows(n):
    shape = (16 * n, 16 * n)
    row, col = iota2(shape, 0), iota2(shape, 1)
    q, rest = row // (4 * n), row % (4 * n)
    return (col == (rest // 4) * 16 + q * 4 + rest % 4).astype(BF16)


def scatter_rows(n):
    shape = (16 * n, 16 * n)
    row, col = iota2(shape, 0), iota2(shape, 1)
    q, rest = col // (4 * n), col % (4 * n)
    return (row == (rest // 4) * 16 + q * 4 + rest % 4).astype(BF16)


def piece_factor(piece):
    partial = jnp.sum(piece * piece, axis=1, keepdims=True)
    same = (iota2((16, 16), 0) % 4 == iota2((16, 16), 1) % 4).astype(F32)
    total = jnp.dot(
        same,
        jnp.broadcast_to(partial, (16, 128)),
        preferred_element_type=F32,
        precision=lax.Precision.HIGHEST,
    )
    return lax.rsqrt(total[:, :1] / D + EPS)


def kernel(
    res_ref, gain1_ref, gain2_ref, mgain_ref, ggain_ref, bias_ref, rate_ref, skip_ref,
    tapi_ref, tapw_ref, tapr_ref, bufi_ref, bufw_ref, bufr_ref,
    fg_ref, fl_ref, fd_ref, sg_ref, sl_ref, sd_ref,
    pg_ref, pi_ref, pw_ref, pr_ref, ps_ref, po_ref, scan_ref,
    out_ref, state_ref,
    msg, recv_r, wg1, wl1, wd1, wg2, wl2, wd2,
    ag1, ag2, perm, permt, hid, psend, znear, ry1, rn1, zs1, rz1, ry2, rn2, zs2, rz2,
    send_f, recv_f, recv_o, send_o, send_q, recv_q,
    pgv, piv, pwv, prv, psv, pov, scan_f, scan_b, xrow, gsplit,
    loc_sem, s_all, r_t, s_w, r_wx, r_wc, r_ag, r_y, r_z,
):
    kv = lax.axis_index("kv")
    t = lax.axis_index("tp")
    z, y = kv // NY, kv % NY
    core = t % 2

    def zpeer(d):
        return lax.rem(z + d, NZ)

    def ypeer(d):
        return lax.rem(y + d, NY)

    def tpeer(d):
        return lax.rem(t + d, NT)

    def rcopy(src, dst, ssem, rsem, dev):
        return pltpu.make_async_remote_copy(
            src_ref=src, dst_ref=dst, send_sem=ssem, recv_sem=rsem, device_id=dev, device_id_type=MESH
        )

    def wait_recv(block, rsem):
        rcopy(block, block, s_all.at[0], rsem, (kv, tpeer(1))).wait_recv()

    def wait_send(block, ssem):
        rcopy(block, block, ssem, r_t.at[0], (kv, tpeer(1))).wait_send()

    def local(src, dst, k):
        copy = pltpu.make_async_copy(src, dst, loc_sem.at[k])
        copy.start()
        return copy

    for src, dst in ((fg_ref, wg1), (fl_ref, wl1), (fd_ref, wd1)):
        local(src, dst.at[t], 1)

    barrier = pltpu.get_barrier_semaphore()
    peers = [(zpeer(d) * NY + y, t) for d in range(1, NZ)]
    peers += [(z * NY + ypeer(d), t) for d in range(1, NY)]
    peers += [(kv, tpeer(d)) for d in range(1, NT)]
    for dev in peers:
        pl.semaphore_signal(barrier, inc=1, device_id=dev, device_id_type=MESH)

    def as_row(ref):
        wide = ref[...].astype(F32)
        return jnp.concatenate([wide[k : k + 1] for k in range(wide.shape[0])], axis=1)

    row, col = iota2((128, 32), 0), iota2((128, 32), 1)
    give = ((col == (row // 16) * 4 + row % 16) & (row % 16 < 4)).astype(BF16)
    kind = (iota2((128, GROUP), 0) % 16) // 4
    body = dot(give, res_ref[...])
    body = jnp.where(kind == 1, as_row(gain1_ref), jnp.where(kind == 2, as_row(gain2_ref), body))
    msg[...] = body.astype(BF16).reshape(NT, 16, GROUP)
    recv_r[t] = msg[t]

    pl.semaphore_wait(barrier, len(peers))

    def exchange_tp(block, dst, k):
        for d in range(1, NT):
            tt = tpeer(d)
            rcopy(block(tt), dst, s_all.at[k], r_t.at[k], (kv, tt)).start()

    exchange_tp(lambda tt: msg.at[tt], recv_r.at[t], 0)

    def start_weights(k, src, dst):
        for j in range(1, 4):
            tt = lax.rem(t + 2 * j, NT)
            rcopy(src, dst.at[t], s_w.at[k], r_wx.at[k], (kv, tt)).start()
        rcopy(src, dst.at[t], s_w.at[k], r_wc.at[k], (kv, t + 1 - 2 * core)).start()

    def forward_weights(k, dst):
        wait_recv(dst.at[pl.ds(0, 3)], r_wx.at[k])
        for j in range(1, 4):
            ss = lax.rem(t - 2 * j + NT, NT)
            rcopy(dst.at[ss], dst.at[ss], s_w.at[k], r_wc.at[k], (kv, t + 1 - 2 * core)).start()

    def finish_weights(k, dst):
        wait_recv(dst.at[pl.ds(0, 4)], r_wc.at[k])
        wait_send(dst.at[pl.ds(0, 7)], s_w.at[k])

    for k, (src, dst) in enumerate(((fg_ref, wg1), (fl_ref, wl1), (fd_ref, wd1))):
        start_weights(k, src, dst)

    l_mix = [
        local(pg_ref, pgv, 3), local(pi_ref, piv, 4), local(pw_ref, pwv, 5), local(pr_ref, prv, 6),
        local(ps_ref, psv, 7), local(po_ref, pov, 8), local(scan_ref, scan_f, 9),
    ]
    for src, dst in ((sg_ref, wg2), (sl_ref, wl2), (sd_ref, wd2)):
        local(src, dst.at[t], 2)

    perm[...] = gather_rows(NKV)
    permt[...] = scatter_rows(NKV)
    wait_recv(recv_r.at[pl.ds(0, NT - 1)], r_t.at[0])

    row, col = iota2((48, 64), 0), iota2((48, 64), 1)
    pick = (col == ((row % 16) // 4) * 16 + (row // 16) * 4 + row % 4).astype(BF16)
    halves = []
    for h in range(2):
        block = jnp.concatenate([recv_r[2 * q + h] for q in range(4)], axis=0)
        halves.append(dot(pick, block))
    both = jnp.concatenate(halves, axis=1)
    res1 = both[0:16]
    gsplit[...] = both[16:48]

    ag_order = ((2, 0), (6, 0), (0, 1), (0, 3), (3, 0), (5, 0), (0, 2), (4, 0))

    def gather_send(ag, slot, f, d, e, dev):
        k = ag_order.index((d, e)) if (d, e) in ag_order else 8
        rcopy(ag.at[slot], ag.at[slot], s_all.at[4 + f], r_ag.at[f, k], (dev, t)).start()

    def start_gather(ag, f):
        for d in (4, 3, 5, 2, 6, 1, 7):
            gather_send(ag, kv, f, d, 0, zpeer(d) * NY + y)
        for e in (2, 1, 3):
            gather_send(ag, kv, f, 0, e, z * NY + ypeer(e))

    def forward_gather(ag, f):
        for k, (d, e) in enumerate(ag_order):
            slot = lax.rem(z - d + NZ, NZ) * NY + lax.rem(y - e + NY, NY)
            wait_recv(ag.at[slot], r_ag.at[f, k])
            if e == 0:
                for ee in (2, 1, 3):
                    gather_send(ag, slot, f, d, ee, z * NY + ypeer(ee))
            else:
                for dd in (1, 7):
                    gather_send(ag, slot, f, dd, e, zpeer(dd) * NY + y)

    def finish_gather(ag, f):
        wait_recv(ag.at[pl.ds(0, 23)], r_ag.at[f, 8])
        wait_send(ag.at[pl.ds(0, 31)], s_all.at[4 + f])

    def feed_forward(ag, wg, wl, wd):
        flat = ag[...].reshape(16 * NKV, QW)
        lhs = dot(perm[...], flat).astype(BF16)
        gate, lift = None, None
        for s in range(NT):
            q, h = s // 2, s % 2
            part = lhs[128 * q : 128 * q + 128, 256 * h : 256 * h + 256]
            g, u = dot_nt(part, wg[s]), dot_nt(part, wl[s])
            gate = g if gate is None else gate + g
            lift = u if lift is None else lift + u
        hidden = (gate * jax.nn.sigmoid(gate) * lift).astype(BF16)
        for s in range(NT):
            q, h = s // 2, s % 2
            hid[128 * q : 128 * q + 128, 256 * h : 256 * h + 256] = dot(hidden, wd[s]).astype(BF16)
        psend[...] = dot(permt[...], hid[...]).astype(BF16).reshape(NKV, 16, QW)

    y_order = (4, 3, 5, 2, 6, 0)

    def reduce_send_y(block, ry, f, d):
        for e in (2, 1, 3):
            yy = ypeer(e)
            k = y_order.index(d)
            rcopy(block(yy), ry.at[d, e], s_all.at[6 + f], r_y.at[f, k], (z * NY + yy, t)).start()

    def reduce_start(ry, rn, f):
        for d in (4, 3, 5, 2, 6):
            zz = zpeer(d)
            reduce_send_y(lambda yy: psend.at[zz * NY + yy], ry, f, d)
            if d == 4:
                for k, dd in enumerate((1, 7)):
                    near = zpeer(dd)
                    rcopy(
                        psend.at[pl.ds(near * NY, NY)], rn.at[pl.ds(NY * k, NY)], s_all.at[6 + f], r_z.at[f, 0],
                        (near * NY + y, t),
                    ).start()

    def reduce_finish(ry, rn, zs, rz, f):
        wait_recv(rn.at[pl.ds(0, 2 * NY)], r_z.at[f, 0])
        near = psend[pl.ds(z * NY, NY)].astype(F32) + rn[0:NY].astype(F32) + rn[NY : 2 * NY].astype(F32)
        znear[...] = near.astype(BF16)
        reduce_send_y(lambda yy: znear.at[yy], ry, f, 0)

        def with_y(total, d):
            wait_recv(ry.at[d, pl.ds(1, NY - 1)], r_y.at[f, y_order.index(d)])
            for e in range(1, NY):
                total = total + ry[d, e].astype(F32)
            return total

        for d in (4, 3, 5, 2, 6):
            zz = zpeer(d)
            zs[d] = with_y(psend[zz * NY + y].astype(F32), d).astype(BF16)
            rcopy(zs.at[d], rz.at[d], s_all.at[6 + f], r_z.at[f, 1], (zz * NY + y, t)).start()
        own = with_y(znear[y].astype(F32), 0)
        wait_recv(rz.at[pl.ds(0, 5)], r_z.at[f, 1])
        for d in (2, 6, 3, 5, 4):
            own = own + rz[d].astype(F32)
        wait_send(psend.at[pl.ds(0, 31)], s_all.at[6 + f])
        return own

    ag1[kv] = (res1 * piece_factor(res1) * gsplit[0:16]).astype(BF16)
    start_gather(ag1, 0)
    forward_gather(ag1, 0)
    for k, dst in enumerate((wg1, wl1, wd1)):
        forward_weights(k, dst)
    finish_gather(ag1, 0)
    pltpu.make_async_copy(wg1.at[pl.ds(0, 3)], wg1.at[pl.ds(0, 3)], loc_sem.at[1]).wait()
    for k, dst in enumerate((wg1, wl1, wd1)):
        finish_weights(k, dst)
    feed_forward(ag1, wg1, wl1, wd1)
    reduce_start(ry1, rn1, 0)
    start_weights(3, sg_ref, wg2)
    start_weights(4, sl_ref, wl2)
    for copy in l_mix:
        copy.wait()
    scan_b[...] = scan_f[...].astype(BF16)
    branch = reduce_finish(ry1, rn1, zs1, rz1, 0)
    first = (res1 + 0.5 * branch).astype(BF16).astype(F32)

    row, col = iota2((16, 16), 0), iota2((16, 16), 1)
    mixer_gain = jnp.concatenate(
        [dot((col == (row // 4) * 4 + j).astype(BF16), mgain_ref[...]) for j in range(4)], axis=1
    )
    send_f[...] = (first * piece_factor(first) * mixer_gain).astype(BF16)
    exchange_tp(lambda tt: send_f, recv_f.at[t], 1)
    recv_f[t] = send_f[...]
    perm8 = gather_rows(NT)
    wait_recv(recv_f.at[pl.ds(0, NT - 1)], r_t.at[1])
    rows = dot(perm8, recv_f[...].reshape(128, QW)).astype(BF16)
    for q in range(4):
        xrow[:, QW * q : QW * q + QW] = rows[32 * q : 32 * q + 32]
    mixed_in = xrow[...]

    def project(w):
        return dot(mixed_in, w[...]).astype(BF16).astype(F32)

    gate_z, input_new = project(pgv), project(piv)
    write_new, read_new, step_raw4 = project(pwv), project(prv), dot_nt(mixed_in, psv[...]).astype(BF16).astype(F32)

    def silu(v):
        return v * jax.nn.sigmoid(v)

    def short_conv(tap_ref, buf_ref, newest):
        taps = tap_ref[...].astype(F32)
        total = newest * taps[3:4]
        for k in range(3):
            total = total + buf_ref[k].astype(F32) * taps[k : k + 1]
        return silu(total)

    xc = short_conv(tapi_ref, bufi_ref, input_new)
    bc = short_conv(tapw_ref, bufw_ref, write_new)
    rc = short_conv(tapr_ref, bufr_ref, read_new)
    lane_head = iota2((SEQ, GROUP), 1) // HEAD_DIM
    step_raw = jnp.zeros((SEQ, GROUP), F32)
    for h in range(4):
        step_raw = jnp.where(lane_head == h, step_raw4[:, h : h + 1], step_raw)
    head_row = iota2((1, GROUP), 1) // HEAD_DIM

    def per_head(ref):
        wide = jnp.full((1, GROUP), ref[0], F32)
        for h in range(1, 4):
            wide = jnp.where(head_row == h, ref[h], wide)
        return wide

    pre = step_raw + per_head(bias_ref)
    step = jnp.maximum(pre, 0.0) + jnp.log1p(jnp.exp(-jnp.abs(pre)))
    retain = jnp.exp(-step * jnp.exp(per_head(rate_ref)))
    u = step * xc
    rcb = rc.astype(BF16)
    sub = iota2((8, GROUP), 0)
    reads = []
    for g in range(4):
        acc = jnp.zeros((8, GROUP), F32)
        for j in range(8):
            b = 8 * g + j
            got = dot_nt(rcb[8 * g : 8 * g + 8], scan_b[b])
            acc = jnp.where(sub == j, got, acc)
        reads.append(acc)
    read = jnp.concatenate(reads, axis=0)
    head = retain * read + u * jnp.sum(bc * rc, axis=1, keepdims=True) + per_head(skip_ref) * xc
    gated = head.astype(BF16).astype(F32) * silu(gate_z)
    gated = gated * lax.rsqrt(jnp.mean(gated * gated, axis=1, keepdims=True) + EPS) * as_row(ggain_ref)
    part = dot(gated.astype(BF16), pov[...]).astype(BF16)
    stacked = jnp.concatenate([part[:, QW * q : QW * q + QW] for q in range(4)], axis=0)
    send_o[...] = dot(scatter_rows(NT), stacked).astype(BF16).reshape(NT, 16, QW)
    exchange_tp(lambda tt: send_o.at[tt], recv_o.at[t], 2)
    recv_o[t] = send_o[t]
    pltpu.make_async_copy(wg2.at[pl.ds(0, 3)], wg2.at[pl.ds(0, 3)], loc_sem.at[2]).wait()
    start_weights(5, sd_ref, wd2)
    u_cols = jnp.transpose(u)
    for b in range(SEQ):
        for h in range(4):
            rows_h = slice(HEAD_DIM * h, HEAD_DIM * h + HEAD_DIM)
            keep = jnp.broadcast_to(retain[b : b + 1, HEAD_DIM * h : HEAD_DIM * h + 1], (HEAD_DIM, STATE))
            scan_f[b, rows_h, :] = keep * scan_f[b, rows_h, :] + u_cols[rows_h, b : b + 1] * bc[b : b + 1]
    l_state = local(scan_f, state_ref, 0)
    wait_recv(recv_o.at[pl.ds(0, NT - 1)], r_t.at[2])
    mixed = first
    for k in range(NT):
        mixed = mixed + recv_o[k].astype(F32)
    res2 = mixed.astype(BF16).astype(F32)

    ag2[kv] = (res2 * piece_factor(res2) * gsplit[16:32]).astype(BF16)
    start_gather(ag2, 1)
    forward_weights(3, wg2)
    forward_weights(4, wl2)
    forward_gather(ag2, 1)
    forward_weights(5, wd2)
    finish_gather(ag2, 1)
    for k, dst in enumerate((wg2, wl2, wd2)):
        finish_weights(3 + k, dst)
    feed_forward(ag2, wg2, wl2, wd2)
    reduce_start(ry2, rn2, 1)
    branch = reduce_finish(ry2, rn2, zs2, rz2, 1)
    final = (res2 + 0.5 * branch).astype(BF16)

    row, col = iota2((64, 16), 0), iota2((64, 16), 1)
    spread = ((col == (row // 16) * 4 + row % 16) & (row % 16 < 4)).astype(BF16)
    for h in range(2):
        block = dot(spread, final[:, 256 * h : 256 * h + 256]).astype(BF16).reshape(4, 16, 256)
        for q in range(4):
            send_q[2 * q + h] = block[q]
    exchange_tp(lambda tt: send_q.at[tt], recv_q.at[t], 3)
    recv_q[t] = send_q[t]
    row, col = iota2((32, 128), 0), iota2((32, 128), 1)
    pick32 = (col == (row // 4) * 16 + row % 4).astype(BF16)
    wait_recv(recv_q.at[pl.ds(0, NT - 1)], r_t.at[3])
    out_ref[...] = dot(pick32, recv_q[...].reshape(128, 256)).astype(BF16)

    l_state.wait()
    for k, block in enumerate((recv_r, recv_f, recv_o, recv_q)):
        wait_send(block.at[pl.ds(0, NT - 1)], s_all.at[k])


def per_device(
    residual, first_gain, first_gate, first_lift, first_down, mixer_gain,
    proj_gate, proj_input, proj_write, proj_read, proj_step,
    step_bias, rate_log, skip_gain, taps_input, taps_write, taps_read,
    buffer_input, buffer_write, buffer_read, scan_state, group_gain, proj_output,
    second_gain, second_gate, second_lift, second_down,
):
    scan = scan_state.reshape(SEQ, GROUP, STATE)
    vm = pl.BlockSpec(memory_space=pltpu.VMEM)
    sm = pl.BlockSpec(memory_space=pltpu.SMEM)
    anym = pl.BlockSpec(memory_space=pl.ANY)
    hid_cols = first_gate.shape[1]
    dma = pltpu.SemaphoreType.DMA
    out, state = pl.pallas_call(
        kernel,
        out_shape=(
            pltpu.VMEM((SEQ, GROUP), BF16),
            pltpu.VMEM((SEQ, GROUP, STATE), F32),
        ),
        in_specs=[vm] * 5 + [sm] * 3 + [vm] * 6 + [anym] * 13,
        out_specs=(vm, anym),
        scratch_shapes=[
            pltpu.VMEM((NT, 16, GROUP), BF16),
            pltpu.VMEM((NT, 16, GROUP), BF16),
            *[pltpu.VMEM((NT, hid_cols, 256), BF16), pltpu.VMEM((NT, hid_cols, 256), BF16), pltpu.VMEM((NT, hid_cols, 256), BF16)] * 2,
            pltpu.VMEM((NKV, 16, QW), BF16),
            pltpu.VMEM((NKV, 16, QW), BF16),
            pltpu.VMEM((16 * NKV, 16 * NKV), BF16),
            pltpu.VMEM((16 * NKV, 16 * NKV), BF16),
            pltpu.VMEM((512, QW), BF16),
            pltpu.VMEM((NKV, 16, QW), BF16),
            pltpu.VMEM((NY, 16, QW), BF16),
            *[pltpu.VMEM((NZ, NY, 16, QW), BF16), pltpu.VMEM((2 * NY, 16, QW), BF16), pltpu.VMEM((NZ, 16, QW), BF16), pltpu.VMEM((NZ, 16, QW), BF16)] * 2,
            pltpu.VMEM((16, QW), BF16),
            pltpu.VMEM((NT, 16, QW), BF16),
            pltpu.VMEM((NT, 16, QW), BF16),
            pltpu.VMEM((NT, 16, QW), BF16),
            pltpu.VMEM((NT, 16, GROUP), BF16),
            pltpu.VMEM((NT, 16, GROUP), BF16),
            pltpu.VMEM((D, 256), BF16),
            pltpu.VMEM((D, 256), BF16),
            pltpu.VMEM((D, 128), BF16),
            pltpu.VMEM((D, 128), BF16),
            pltpu.VMEM((4, D), BF16),
            pltpu.VMEM((256, D), BF16),
            pltpu.VMEM((SEQ, GROUP, STATE), F32),
            pltpu.VMEM((SEQ, GROUP, STATE), BF16),
            pltpu.VMEM((SEQ, D), BF16),
            pltpu.VMEM((32, QW), F32),
            dma((10,)), dma((8,)), dma((4,)),
            dma((6,)), dma((6,)), dma((6,)),
            dma((2, 9)), dma((2, 6)), dma((2, 2)),
        ],
        compiler_params=pltpu.CompilerParams(
            collective_id=0, has_side_effects=True, vmem_limit_bytes=56 * 1024 * 1024
        ),
        name="layer",
    )(
        residual, first_gain.reshape(2, 128), second_gain.reshape(2, 128), mixer_gain.reshape(16, 128),
        group_gain.reshape(2, 128), step_bias, rate_log, skip_gain,
        taps_input, taps_write, taps_read,
        buffer_input.transpose(1, 0, 2), buffer_write.transpose(1, 0, 2), buffer_read.transpose(1, 0, 2),
        first_gate.T, first_lift.T, first_down, second_gate.T, second_lift.T, second_down,
        proj_gate, proj_input, proj_write, proj_read, proj_step.T, proj_output, scan,
    )
    return out, state.reshape(scan_state.shape)


def solution(mesh):
    placed = (
        P("kv", "tp"), P("tp"), P("tp", "kv"), P("tp", "kv"), P("kv", "tp"), P(),
        P(None, "tp"), P(None, "tp"), P(None, "tp"), P(None, "tp"), P(None, "tp"),
        P("tp"), P("tp"), P("tp"), P(None, "tp"), P(None, "tp"), P(None, "tp"),
        P("kv", None, "tp"), P("kv", None, "tp"), P("kv", None, "tp"), P("kv", "tp", None, None),
        P("tp"), P("tp", None), P("tp"), P("tp", "kv"), P("tp", "kv"), P("kv", "tp"),
    )
    return jax.shard_map(
        per_device,
        mesh=mesh,
        in_specs=placed,
        out_specs=(P("kv", "tp"), P("kv", "tp", None, None)),
        check_vma=False,
    )
```

time: 118 us -> 79.8 us (0.68)
  local copies, waits for them, and re-layouts: 17.1 us -> 2.62 us
  other arithmetic: 12.2 us -> 0 us
  Pallas kernels: 87 us -> 76.4 us
    pallas_call x1, Pallas kernels: 87 us -> 76.4 us  [per_device(): pl.pallas_call(kernel, out_shape=(pltpu.VMEM((SEQ, GROUP), BF16), pltpu.V...]
    unnamed x8 -> x2, local copies, waits for them, and re-layouts: 8.95 us -> 2.62 us
    add x1 -> x0, other arithmetic: 5.82 us -> none  [per_device(): retain[:, ::HEAD_DIM][:, :, None, None] * scan_state]
    broadcast_in_dim x7 -> x0, local copies, waits for them, and re-layouts: 3.5 us -> none  [the longest x1 0.72 us: per_device(): jnp.repeat(rate_log, HEAD_DIM)]
    convert_element_type x4 -> x0, other arithmetic: 2.81 us -> none  [the longest x3 2.05 us: per_device(): tap[None, :3, :].astype(F32)]
    reshape x3 -> x0, local copies, waits for them, and re-layouts: 2.04 us -> none  [the longest x2 1.31 us: per_device(): mgain = jnp.repeat(mixer_gain.astype(F32).reshape(4, QW), RPT, axis=0)]
    reduce_sum x2 -> x0, other arithmetic: 1.59 us -> none  [per_device(): jnp.sum(buf.astype(F32) * tap[None, :3, :].astype(F32), axis=1)]
    concatenate x2 -> x0, other arithmetic: 1.32 us -> none  [the longest x1 0.7 us: per_device(): jnp.concatenate([residual.reshape(NT, RPT, GROUP), jnp.broadcast_to(first...]
where the time goes in v2:
time: 79.8 us; the launch traced here: 79.7 us
  Pallas kernels  76.4 us (96%)
  local copies, waits for them, and re-layouts  2.62 us (3%)
    pallas_call x1, Pallas kernels, per_device(): pl.pallas_call(kernel, out_shape=(pltpu.VMEM((SEQ, GROUP), BF16), pltpu.V...  76.4 us
    unnamed x2, local copies, waits for them, and re-layouts  2.62 us

profile of v2, /device:TPU:1, one launch (start us, length us, event | category | flops | bytes accessed | tf_op | source)
XLA Modules:
  0.0 79.7 jit_solution(15359486505112543408)
XLA Ops:
  0.6 76.4 %layer.1 = (bf16[32,256]{1,0:T(8,128)(2,1)S(1)}, f32[32,256,128]{2,1,0:T(8,128)S(1)}) custom-call(bf16[32,256]{1,0:T(8,128)(2,1)} %res_ref.1, bf16[2,128]{1,0:T(2,128)(2,1)} %bitcast.25, bf16[2,128]{1,0:T(2,128)(2,1)} %bitcast.26, bf16[16,128]{1,0:T(8,128)(2,1)} %bitcast.24, bf16[2,128]{1,0:T(2,128)(2,1)} %bitcast.27, f32[4]{0:T(128)} %bias_ref.1, ...), custom_call_target="tpu_custom_call" | custom-call | tf_op jit(solution)/shard_map/layer/pallas_call | solution.py:407
  77.1 0.6 copy.31
  77.7 2.0 %copy.32 = f32[32,4,64,128]{3,2,1,0:T(8,128)} copy(f32[32,4,64,128]{3,2,1,0:T(8,128)S(1)} %bitcast.14) | data formatting | bytes 8388608

commit v3 on v2

--- a/solution.py
+++ b/solution.py
@@ -58,18 +58,21 @@
     return lax.rsqrt(total[:, :1] / D + EPS)
 
 
-def kernel(
-    res_ref, gain1_ref, gain2_ref, mgain_ref, ggain_ref, bias_ref, rate_ref, skip_ref,
-    tapi_ref, tapw_ref, tapr_ref, bufi_ref, bufw_ref, bufr_ref,
-    fg_ref, fl_ref, fd_ref, sg_ref, sl_ref, sd_ref,
-    pg_ref, pi_ref, pw_ref, pr_ref, ps_ref, po_ref, scan_ref,
-    out_ref, state_ref,
-    msg, recv_r, wg1, wl1, wd1, wg2, wl2, wd2,
-    ag1, ag2, perm, permt, hid, psend, znear, ry1, rn1, zs1, rz1, ry2, rn2, zs2, rz2,
-    send_f, recv_f, recv_o, send_o, send_q, recv_q,
-    pgv, piv, pwv, prv, psv, pov, scan_f, scan_b, xrow, gsplit,
-    loc_sem, s_all, r_t, s_w, r_wx, r_wc, r_ag, r_y, r_z,
-):
+def kernel(*refs):
+    small_in, refs = refs[:14], refs[14:]
+    (fg_ref, fl_ref, fd_ref, sg_ref, sl_ref, sd_ref), refs = refs[:6], refs[6:]
+    (pg_ref, pi_ref, pw_ref, pr_ref, ps_ref, po_ref, scan_ref), refs = refs[:7], refs[7:]
+    (out_ref, state_ref), refs = refs[:2], refs[2:]
+    small, refs = refs[:14], refs[14:]
+    res_ref, gain1_ref, gain2_ref, mgain_ref, ggain_ref, bias_ref, rate_ref, skip_ref = small[:8]
+    tapi_ref, tapw_ref, tapr_ref, bufi_ref, bufw_ref, bufr_ref = small[8:]
+    (
+        msg, recv_r, wg1, wl1, wd1, wg2, wl2, wd2,
+        ag1, ag2, perm, permt, hid, psend, znear, ry1, rn1, zs1, rz1, ry2, rn2, zs2, rz2,
+        send_f, recv_f, recv_o, send_o, send_q, recv_q,
+        pgv, piv, pwv, prv, psv, pov, scan_f, scan_b, xrow, gsplit,
+        loc_sem, s_all, r_t, s_w, r_wx, r_wo, r_wc, r_ag, r_y, r_z, in_sem, ready,
+    ) = refs
     kv = lax.axis_index("kv")
     t = lax.axis_index("tp")
     z, y = kv // NY, kv % NY
@@ -100,15 +103,21 @@
         copy.start()
         return copy
 
+    barrier = pltpu.get_barrier_semaphore()
+    peers = [(kv, tpeer(d)) for d in range(1, NT)]
+    peers += [(zpeer(d) * NY + y, t) for d in (1, 7)]
+    peers += [(z * NY + ypeer(d), t) for d in range(1, NY)]
+    for dev in peers:
+        pl.semaphore_signal(barrier, inc=1, device_id=dev, device_id_type=MESH)
+    l_small = []
+    for k in range(14):
+        copy = pltpu.make_async_copy(small_in[k], small[k], in_sem.at[k])
+        copy.start()
+        l_small.append(copy)
     for src, dst in ((fg_ref, wg1), (fl_ref, wl1), (fd_ref, wd1)):
         local(src, dst.at[t], 1)
-
-    barrier = pltpu.get_barrier_semaphore()
-    peers = [(zpeer(d) * NY + y, t) for d in range(1, NZ)]
-    peers += [(z * NY + ypeer(d), t) for d in range(1, NY)]
-    peers += [(kv, tpeer(d)) for d in range(1, NT)]
-    for dev in peers:
-        pl.semaphore_signal(barrier, inc=1, device_id=dev, device_id_type=MESH)
+    for k in range(3):
+        l_small[k].wait()
 
     def as_row(ref):
         wide = ref[...].astype(F32)
@@ -130,18 +139,33 @@
             rcopy(block(tt), dst, s_all.at[k], r_t.at[k], (kv, tt)).start()
 
     exchange_tp(lambda tt: msg.at[tt], recv_r.at[t], 0)
+    for d in (1, 7):
+        pl.semaphore_signal(ready.at[0], inc=1, device_id=(zpeer(d) * NY + y, t), device_id_type=MESH)
+
+    partner = t + 1 - 2 * core
+    left, right, across = lax.rem(t + NT - 2, NT), lax.rem(t + 2, NT), lax.rem(t + 4, NT)
+    cuts = (fg_ref.shape[0], 0, 96)
 
     def start_weights(k, src, dst):
-        for j in range(1, 4):
-            tt = lax.rem(t + 2 * j, NT)
+        for tt in (right, left):
             rcopy(src, dst.at[t], s_w.at[k], r_wx.at[k], (kv, tt)).start()
-        rcopy(src, dst.at[t], s_w.at[k], r_wc.at[k], (kv, t + 1 - 2 * core)).start()
+        rcopy(src, dst.at[t], s_w.at[k], r_wc.at[k], (kv, partner)).start()
+
+    def relay_weights(k, dst):
+        wait_recv(dst.at[pl.ds(0, 2)], r_wx.at[k])
+        cut, depth = cuts[k % 3], dst.shape[1]
+        if cut > 0:
+            part = dst.at[left, pl.ds(0, cut)]
+            rcopy(part, part, s_w.at[k], r_wo.at[k], (kv, right)).start()
+        if cut < depth:
+            part = dst.at[right, pl.ds(cut, depth - cut)]
+            rcopy(part, part, s_w.at[k], r_wo.at[k], (kv, left)).start()
+        for ss in (left, right):
+            rcopy(dst.at[ss], dst.at[ss], s_w.at[k], r_wc.at[k], (kv, partner)).start()
 
     def forward_weights(k, dst):
-        wait_recv(dst.at[pl.ds(0, 3)], r_wx.at[k])
-        for j in range(1, 4):
-            ss = lax.rem(t - 2 * j + NT, NT)
-            rcopy(dst.at[ss], dst.at[ss], s_w.at[k], r_wc.at[k], (kv, t + 1 - 2 * core)).start()
+        wait_recv(dst.at[0], r_wo.at[k])
+        rcopy(dst.at[across], dst.at[across], s_w.at[k], r_wc.at[k], (kv, partner)).start()
 
     def finish_weights(k, dst):
         wait_recv(dst.at[pl.ds(0, 4)], r_wc.at[k])
@@ -157,10 +181,16 @@
     for src, dst in ((sg_ref, wg2), (sl_ref, wl2), (sd_ref, wd2)):
         local(src, dst.at[t], 2)
 
+    pl.semaphore_wait(ready.at[0], 2)
+    for d in (2, 6):
+        pl.semaphore_signal(ready.at[1], inc=1, device_id=(zpeer(d) * NY + y, t), device_id_type=MESH)
     perm[...] = gather_rows(NKV)
     permt[...] = scatter_rows(NKV)
+    for k in range(3, 14):
+        l_small[k].wait()
     wait_recv(recv_r.at[pl.ds(0, NT - 1)], r_t.at[0])
 
+    pl.semaphore_wait(ready.at[1], 2)
     row, col = iota2((48, 64), 0), iota2((48, 64), 1)
     pick = (col == ((row % 16) // 4) * 16 + (row // 16) * 4 + row % 4).astype(BF16)
     halves = []
@@ -183,8 +213,11 @@
         for e in (2, 1, 3):
             gather_send(ag, kv, f, 0, e, z * NY + ypeer(e))
 
-    def forward_gather(ag, f):
+    def forward_gather(ag, f, between=()):
         for k, (d, e) in enumerate(ag_order):
+            for at, step, weights in between:
+                if at == k:
+                    relay_weights(step, weights)
             slot = lax.rem(z - d + NZ, NZ) * NY + lax.rem(y - e + NY, NY)
             wait_recv(ag.at[slot], r_ag.at[f, k])
             if e == 0:
@@ -198,7 +231,7 @@
         wait_recv(ag.at[pl.ds(0, 23)], r_ag.at[f, 8])
         wait_send(ag.at[pl.ds(0, 31)], s_all.at[4 + f])
 
-    def feed_forward(ag, wg, wl, wd):
+    def feed_forward(ag, wg, wl, wd, k):
         flat = ag[...].reshape(16 * NKV, QW)
         lhs = dot(perm[...], flat).astype(BF16)
         gate, lift = None, None
@@ -208,6 +241,7 @@
             g, u = dot_nt(part, wg[s]), dot_nt(part, wl[s])
             gate = g if gate is None else gate + g
             lift = u if lift is None else lift + u
+        finish_weights(k + 2, wd)
         hidden = (gate * jax.nn.sigmoid(gate) * lift).astype(BF16)
         for s in range(NT):
             q, h = s // 2, s % 2
@@ -234,7 +268,7 @@
                         (near * NY + y, t),
                     ).start()
 
-    def reduce_finish(ry, rn, zs, rz, f):
+    def reduce_finish(ry, rn, zs, rz, f, between=()):
         wait_recv(rn.at[pl.ds(0, 2 * NY)], r_z.at[f, 0])
         near = psend[pl.ds(z * NY, NY)].astype(F32) + rn[0:NY].astype(F32) + rn[NY : 2 * NY].astype(F32)
         znear[...] = near.astype(BF16)
@@ -247,6 +281,9 @@
             return total
 
         for d in (4, 3, 5, 2, 6):
+            for at, step, weights in between:
+                if at == d:
+                    relay_weights(step, weights)
             zz = zpeer(d)
             zs[d] = with_y(psend[zz * NY + y].astype(F32), d).astype(BF16)
             rcopy(zs.at[d], rz.at[d], s_all.at[6 + f], r_z.at[f, 1], (zz * NY + y, t)).start()
@@ -259,21 +296,21 @@
 
     ag1[kv] = (res1 * piece_factor(res1) * gsplit[0:16]).astype(BF16)
     start_gather(ag1, 0)
-    forward_gather(ag1, 0)
+    forward_gather(ag1, 0, ((0, 0, wg1), (0, 1, wl1), (4, 2, wd1)))
     for k, dst in enumerate((wg1, wl1, wd1)):
         forward_weights(k, dst)
+    for k, (src, dst) in enumerate(((sg_ref, wg2), (sl_ref, wl2), (sd_ref, wd2))):
+        start_weights(3 + k, src, dst)
     finish_gather(ag1, 0)
     pltpu.make_async_copy(wg1.at[pl.ds(0, 3)], wg1.at[pl.ds(0, 3)], loc_sem.at[1]).wait()
-    for k, dst in enumerate((wg1, wl1, wd1)):
-        finish_weights(k, dst)
-    feed_forward(ag1, wg1, wl1, wd1)
+    finish_weights(0, wg1)
+    finish_weights(1, wl1)
+    feed_forward(ag1, wg1, wl1, wd1, 0)
     reduce_start(ry1, rn1, 0)
-    start_weights(3, sg_ref, wg2)
-    start_weights(4, sl_ref, wl2)
     for copy in l_mix:
         copy.wait()
     scan_b[...] = scan_f[...].astype(BF16)
-    branch = reduce_finish(ry1, rn1, zs1, rz1, 0)
+    branch = reduce_finish(ry1, rn1, zs1, rz1, 0, ((4, 3, wg2), (4, 4, wl2), (5, 5, wd2)))
     first = (res1 + 0.5 * branch).astype(BF16).astype(F32)
 
     row, col = iota2((16, 16), 0), iota2((16, 16), 1)
@@ -285,6 +322,8 @@
     recv_f[t] = send_f[...]
     perm8 = gather_rows(NT)
     wait_recv(recv_f.at[pl.ds(0, NT - 1)], r_t.at[1])
+    for k, dst in enumerate((wg2, wl2, wd2)):
+        forward_weights(3 + k, dst)
     rows = dot(perm8, recv_f[...].reshape(128, QW)).astype(BF16)
     for q in range(4):
         xrow[:, QW * q : QW * q + QW] = rows[32 * q : 32 * q + 32]
@@ -316,9 +355,10 @@
     head_row = iota2((1, GROUP), 1) // HEAD_DIM
 
     def per_head(ref):
-        wide = jnp.full((1, GROUP), ref[0], F32)
+        values = ref[...]
+        wide = jnp.broadcast_to(values[:, 0:1], (1, GROUP))
         for h in range(1, 4):
-            wide = jnp.where(head_row == h, ref[h], wide)
+            wide = jnp.where(head_row == h, values[:, h : h + 1], wide)
         return wide
 
     pre = step_raw + per_head(bias_ref)
@@ -345,7 +385,6 @@
     exchange_tp(lambda tt: send_o.at[tt], recv_o.at[t], 2)
     recv_o[t] = send_o[t]
     pltpu.make_async_copy(wg2.at[pl.ds(0, 3)], wg2.at[pl.ds(0, 3)], loc_sem.at[2]).wait()
-    start_weights(5, sd_ref, wd2)
     u_cols = jnp.transpose(u)
     for b in range(SEQ):
         for h in range(4):
@@ -361,14 +400,11 @@
 
     ag2[kv] = (res2 * piece_factor(res2) * gsplit[16:32]).astype(BF16)
     start_gather(ag2, 1)
-    forward_weights(3, wg2)
-    forward_weights(4, wl2)
     forward_gather(ag2, 1)
-    forward_weights(5, wd2)
     finish_gather(ag2, 1)
-    for k, dst in enumerate((wg2, wl2, wd2)):
-        finish_weights(3 + k, dst)
-    feed_forward(ag2, wg2, wl2, wd2)
+    finish_weights(3, wg2)
+    finish_weights(4, wl2)
+    feed_forward(ag2, wg2, wl2, wd2, 3)
     reduce_start(ry2, rn2, 1)
     branch = reduce_finish(ry2, rn2, zs2, rz2, 1)
     final = (res2 + 0.5 * branch).astype(BF16)
@@ -399,20 +435,25 @@
     second_gain, second_gate, second_lift, second_down,
 ):
     scan = scan_state.reshape(SEQ, GROUP, STATE)
-    vm = pl.BlockSpec(memory_space=pltpu.VMEM)
-    sm = pl.BlockSpec(memory_space=pltpu.SMEM)
     anym = pl.BlockSpec(memory_space=pl.ANY)
     hid_cols = first_gate.shape[1]
     dma = pltpu.SemaphoreType.DMA
+    small = (
+        residual, first_gain.reshape(2, 128), second_gain.reshape(2, 128), mixer_gain.reshape(16, 128),
+        group_gain.reshape(2, 128), step_bias.reshape(1, 4), rate_log.reshape(1, 4), skip_gain.reshape(1, 4),
+        taps_input, taps_write, taps_read,
+        buffer_input.transpose(1, 0, 2), buffer_write.transpose(1, 0, 2), buffer_read.transpose(1, 0, 2),
+    )
     out, state = pl.pallas_call(
         kernel,
         out_shape=(
             pltpu.VMEM((SEQ, GROUP), BF16),
             pltpu.VMEM((SEQ, GROUP, STATE), F32),
         ),
-        in_specs=[vm] * 5 + [sm] * 3 + [vm] * 6 + [anym] * 13,
-        out_specs=(vm, anym),
+        in_specs=[anym] * 27,
+        out_specs=(pl.BlockSpec(memory_space=pltpu.VMEM), anym),
         scratch_shapes=[
+            *[pltpu.VMEM(a.shape, a.dtype) for a in small],
             pltpu.VMEM((NT, 16, GROUP), BF16),
             pltpu.VMEM((NT, 16, GROUP), BF16),
             *[pltpu.VMEM((NT, hid_cols, 256), BF16), pltpu.VMEM((NT, hid_cols, 256), BF16), pltpu.VMEM((NT, hid_cols, 256), BF16)] * 2,
@@ -441,18 +482,15 @@
             pltpu.VMEM((SEQ, D), BF16),
             pltpu.VMEM((32, QW), F32),
             dma((10,)), dma((8,)), dma((4,)),
-            dma((6,)), dma((6,)), dma((6,)),
-            dma((2, 9)), dma((2, 6)), dma((2, 2)),
+            dma((6,)), dma((6,)), dma((6,)), dma((6,)),
+            dma((2, 9)), dma((2, 6)), dma((2, 2)), dma((14,)), pltpu.SemaphoreType.REGULAR((2,)),
         ],
         compiler_params=pltpu.CompilerParams(
             collective_id=0, has_side_effects=True, vmem_limit_bytes=56 * 1024 * 1024
         ),
         name="layer",
     )(
-        residual, first_gain.reshape(2, 128), second_gain.reshape(2, 128), mixer_gain.reshape(16, 128),
-        group_gain.reshape(2, 128), step_bias, rate_log, skip_gain,
-        taps_input, taps_write, taps_read,
-        buffer_input.transpose(1, 0, 2), buffer_write.transpose(1, 0, 2), buffer_read.transpose(1, 0, 2),
+        *small,
         first_gate.T, first_lift.T, first_down, second_gate.T, second_lift.T, second_down,
         proj_gate, proj_input, proj_write, proj_read, proj_step.T, proj_output, scan,
     )

time: 79.8 us -> 74.6 us (0.935)
  Pallas kernels: 76.4 us -> 71.1 us
    pallas_call x1, Pallas kernels: 76.4 us -> 71.1 us  [per_device(): pl.pallas_call(kernel, out_shape=(pltpu.VMEM((SEQ, GROUP), BF16), pltpu.V...]
where the time goes in v3:
time: 74.6 us; the launch traced here: 74.4 us
  Pallas kernels  71.1 us (95%)
  local copies, waits for them, and re-layouts  2.62 us (4%)
    pallas_call x1, Pallas kernels, per_device(): pl.pallas_call(kernel, out_shape=(pltpu.VMEM((SEQ, GROUP), BF16), pltpu.V...  71.1 us
    unnamed x2, local copies, waits for them, and re-layouts  2.62 us

profile of v3, /device:TPU:1, one launch (start us, length us, event | category | flops | bytes accessed | tf_op | source)
XLA Modules:
  0.0 74.4 jit_solution(2374465135140662900)
XLA Ops:
  0.6 71.1 %layer.1 = (bf16[32,256]{1,0:T(8,128)(2,1)S(1)}, f32[32,256,128]{2,1,0:T(8,128)S(1)}) custom-call(bf16[32,256]{1,0:T(8,128)(2,1)} %refs_0_.1, bf16[2,128]{1,0:T(2,128)(2,1)} %bitcast.28, bf16[2,128]{1,0:T(2,128)(2,1)} %bitcast.29, bf16[16,128]{1,0:T(8,128)(2,1)} %bitcast.27, bf16[2,128]{1,0:T(2,128)(2,1)} %bitcast.30, f32[1,4]{1,0:T(1,128)} %bitcast.31, ...), custom_call_target="tpu_custom_call" | custom-call | tf_op jit(solution)/shard_map/layer/pallas_call | solution.py:447
  71.8 0.6 copy.31
  72.4 2.0 %copy.32 = f32[32,4,64,128]{3,2,1,0:T(8,128)} copy(f32[32,4,64,128]{3,2,1,0:T(8,128)S(1)} %bitcast.17) | data formatting | bytes 8388608

commit v4 on v3

--- a/solution.py
+++ b/solution.py
@@ -47,15 +47,11 @@
 
 
 def piece_factor(piece):
-    partial = jnp.sum(piece * piece, axis=1, keepdims=True)
-    same = (iota2((16, 16), 0) % 4 == iota2((16, 16), 1) % 4).astype(F32)
-    total = jnp.dot(
-        same,
-        jnp.broadcast_to(partial, (16, 128)),
-        preferred_element_type=F32,
-        precision=lax.Precision.HIGHEST,
-    )
-    return lax.rsqrt(total[:, :1] / D + EPS)
+    square = piece * piece
+    total = square[:, 0:128] + square[:, 128:256] + square[:, 256:384] + square[:, 384:512]
+    total = total + pltpu.roll(total, 8, 0)
+    total = total + pltpu.roll(total, 4, 0)
+    return lax.rsqrt(jnp.sum(total, axis=1, keepdims=True) / D + EPS)
 
 
 def kernel(*refs):
@@ -68,7 +64,7 @@
     tapi_ref, tapw_ref, tapr_ref, bufi_ref, bufw_ref, bufr_ref = small[8:]
     (
         msg, recv_r, wg1, wl1, wd1, wg2, wl2, wd2,
-        ag1, ag2, perm, permt, hid, psend, znear, ry1, rn1, zs1, rz1, ry2, rn2, zs2, rz2,
+        ag1, ag2, perm, permt, lhs_v, hid, psend, znear, ry1, rn1, zs1, rz1, ry2, rn2, zs2, rz2,
         send_f, recv_f, recv_o, send_o, send_q, recv_q,
         pgv, piv, pwv, prv, psv, pov, scan_f, scan_b, xrow, gsplit,
         loc_sem, s_all, r_t, s_w, r_wx, r_wo, r_wc, r_ag, r_y, r_z, in_sem, ready,
@@ -134,8 +130,9 @@
     pl.semaphore_wait(barrier, len(peers))
 
     def exchange_tp(block, dst, k):
-        for d in range(1, NT):
-            tt = tpeer(d)
+        base = t - core
+        far, right, left = lax.rem(base + 4, NT), lax.rem(base + 2, NT), lax.rem(base + 6, NT)
+        for tt in (far, far + 1, right, left, right + 1, left + 1, base + 1 - core):
             rcopy(block(tt), dst, s_all.at[k], r_t.at[k], (kv, tt)).start()
 
     exchange_tp(lambda tt: msg.at[tt], recv_r.at[t], 0)
@@ -184,8 +181,8 @@
     pl.semaphore_wait(ready.at[0], 2)
     for d in (2, 6):
         pl.semaphore_signal(ready.at[1], inc=1, device_id=(zpeer(d) * NY + y, t), device_id_type=MESH)
-    perm[...] = gather_rows(NKV)
-    permt[...] = scatter_rows(NKV)
+    perm[...] = gather_rows(NT)
+    permt[...] = scatter_rows(NT)
     for k in range(3, 14):
         l_small[k].wait()
     wait_recv(recv_r.at[pl.ds(0, NT - 1)], r_t.at[0])
@@ -205,7 +202,7 @@
 
     def gather_send(ag, slot, f, d, e, dev):
         k = ag_order.index((d, e)) if (d, e) in ag_order else 8
-        rcopy(ag.at[slot], ag.at[slot], s_all.at[4 + f], r_ag.at[f, k], (dev, t)).start()
+        rcopy(ag.at[slot], ag.at[slot], s_all.at[4], r_ag.at[k], (dev, t)).start()
 
     def start_gather(ag, f):
         for d in (4, 3, 5, 2, 6, 1, 7):
@@ -219,7 +216,7 @@
                 if at == k:
                     relay_weights(step, weights)
             slot = lax.rem(z - d + NZ, NZ) * NY + lax.rem(y - e + NY, NY)
-            wait_recv(ag.at[slot], r_ag.at[f, k])
+            wait_recv(ag.at[slot], r_ag.at[k])
             if e == 0:
                 for ee in (2, 1, 3):
                     gather_send(ag, slot, f, d, ee, z * NY + ypeer(ee))
@@ -228,16 +225,18 @@
                     gather_send(ag, slot, f, dd, e, zpeer(dd) * NY + y)
 
     def finish_gather(ag, f):
-        wait_recv(ag.at[pl.ds(0, 23)], r_ag.at[f, 8])
-        wait_send(ag.at[pl.ds(0, 31)], s_all.at[4 + f])
+        wait_recv(ag.at[pl.ds(0, 23)], r_ag.at[8])
+        wait_send(ag.at[pl.ds(0, 31)], s_all.at[4])
 
     def feed_forward(ag, wg, wl, wd, k):
-        flat = ag[...].reshape(16 * NKV, QW)
-        lhs = dot(perm[...], flat).astype(BF16)
+        for g in range(NKV // 8):
+            rows = dot(perm[...], ag[8 * g : 8 * g + 8].reshape(128, QW)).astype(BF16)
+            for q in range(4):
+                lhs_v[q, 32 * g : 32 * g + 32] = rows[32 * q : 32 * q + 32]
         gate, lift = None, None
         for s in range(NT):
             q, h = s // 2, s % 2
-            part = lhs[128 * q : 128 * q + 128, 256 * h : 256 * h + 256]
+            part = lhs_v[q, :, 256 * h : 256 * h + 256]
             g, u = dot_nt(part, wg[s]), dot_nt(part, wl[s])
             gate = g if gate is None else gate + g
             lift = u if lift is None else lift + u
@@ -245,8 +244,11 @@
         hidden = (gate * jax.nn.sigmoid(gate) * lift).astype(BF16)
         for s in range(NT):
             q, h = s // 2, s % 2
-            hid[128 * q : 128 * q + 128, 256 * h : 256 * h + 256] = dot(hidden, wd[s]).astype(BF16)
-        psend[...] = dot(permt[...], hid[...]).astype(BF16).reshape(NKV, 16, QW)
+            out = dot(hidden, wd[s]).astype(BF16)
+            for g in range(NKV // 8):
+                hid[g, 32 * q : 32 * q + 32, 256 * h : 256 * h + 256] = out[32 * g : 32 * g + 32]
+        for g in range(NKV // 8):
+            psend[8 * g : 8 * g + 8] = dot(permt[...], hid[g]).astype(BF16).reshape(8, 16, QW)
 
     y_order = (4, 3, 5, 2, 6, 0)
 
@@ -254,7 +256,7 @@
         for e in (2, 1, 3):
             yy = ypeer(e)
             k = y_order.index(d)
-            rcopy(block(yy), ry.at[d, e], s_all.at[6 + f], r_y.at[f, k], (z * NY + yy, t)).start()
+            rcopy(block(yy), ry.at[d, e], s_all.at[5], r_y.at[k], (z * NY + yy, t)).start()
 
     def reduce_start(ry, rn, f):
         for d in (4, 3, 5, 2, 6):
@@ -264,34 +266,34 @@
                 for k, dd in enumerate((1, 7)):
                     near = zpeer(dd)
                     rcopy(
-                        psend.at[pl.ds(near * NY, NY)], rn.at[pl.ds(NY * k, NY)], s_all.at[6 + f], r_z.at[f, 0],
+                        psend.at[pl.ds(near * NY, NY)], rn.at[pl.ds(NY * k, NY)], s_all.at[5], r_z.at[0],
                         (near * NY + y, t),
                     ).start()
 
     def reduce_finish(ry, rn, zs, rz, f, between=()):
-        wait_recv(rn.at[pl.ds(0, 2 * NY)], r_z.at[f, 0])
-        near = psend[pl.ds(z * NY, NY)].astype(F32) + rn[0:NY].astype(F32) + rn[NY : 2 * NY].astype(F32)
-        znear[...] = near.astype(BF16)
-        reduce_send_y(lambda yy: znear.at[yy], ry, f, 0)
-
         def with_y(total, d):
-            wait_recv(ry.at[d, pl.ds(1, NY - 1)], r_y.at[f, y_order.index(d)])
+            wait_recv(ry.at[d, pl.ds(1, NY - 1)], r_y.at[y_order.index(d)])
             for e in range(1, NY):
                 total = total + ry[d, e].astype(F32)
             return total
 
         for d in (4, 3, 5, 2, 6):
+            zz = zpeer(d)
+            zs[d] = with_y(psend[zz * NY + y].astype(F32), d).astype(BF16)
+            rcopy(zs.at[d], rz.at[d], s_all.at[5], r_z.at[1], (zz * NY + y, t)).start()
+            if d == 4:
+                wait_recv(rn.at[pl.ds(0, 2 * NY)], r_z.at[0])
+                near = psend[pl.ds(z * NY, NY)].astype(F32) + rn[0:NY].astype(F32) + rn[NY : 2 * NY].astype(F32)
+                znear[...] = near.astype(BF16)
+                reduce_send_y(lambda yy: znear.at[yy], ry, f, 0)
             for at, step, weights in between:
                 if at == d:
                     relay_weights(step, weights)
-            zz = zpeer(d)
-            zs[d] = with_y(psend[zz * NY + y].astype(F32), d).astype(BF16)
-            rcopy(zs.at[d], rz.at[d], s_all.at[6 + f], r_z.at[f, 1], (zz * NY + y, t)).start()
         own = with_y(znear[y].astype(F32), 0)
-        wait_recv(rz.at[pl.ds(0, 5)], r_z.at[f, 1])
+        wait_recv(rz.at[pl.ds(0, 5)], r_z.at[1])
         for d in (2, 6, 3, 5, 4):
             own = own + rz[d].astype(F32)
-        wait_send(psend.at[pl.ds(0, 31)], s_all.at[6 + f])
+        wait_send(psend.at[pl.ds(0, 31)], s_all.at[5])
         return own
 
     ag1[kv] = (res1 * piece_factor(res1) * gsplit[0:16]).astype(BF16)
@@ -320,38 +322,17 @@
     send_f[...] = (first * piece_factor(first) * mixer_gain).astype(BF16)
     exchange_tp(lambda tt: send_f, recv_f.at[t], 1)
     recv_f[t] = send_f[...]
-    perm8 = gather_rows(NT)
-    wait_recv(recv_f.at[pl.ds(0, NT - 1)], r_t.at[1])
-    for k, dst in enumerate((wg2, wl2, wd2)):
-        forward_weights(3 + k, dst)
-    rows = dot(perm8, recv_f[...].reshape(128, QW)).astype(BF16)
-    for q in range(4):
-        xrow[:, QW * q : QW * q + QW] = rows[32 * q : 32 * q + 32]
-    mixed_in = xrow[...]
-
-    def project(w):
-        return dot(mixed_in, w[...]).astype(BF16).astype(F32)
-
-    gate_z, input_new = project(pgv), project(piv)
-    write_new, read_new, step_raw4 = project(pwv), project(prv), dot_nt(mixed_in, psv[...]).astype(BF16).astype(F32)
-
     def silu(v):
         return v * jax.nn.sigmoid(v)
 
-    def short_conv(tap_ref, buf_ref, newest):
+    def old_taps(tap_ref, buf_ref):
         taps = tap_ref[...].astype(F32)
-        total = newest * taps[3:4]
-        for k in range(3):
+        total = buf_ref[0].astype(F32) * taps[0:1]
+        for k in range(1, 3):
             total = total + buf_ref[k].astype(F32) * taps[k : k + 1]
-        return silu(total)
-
-    xc = short_conv(tapi_ref, bufi_ref, input_new)
-    bc = short_conv(tapw_ref, bufw_ref, write_new)
-    rc = short_conv(tapr_ref, bufr_ref, read_new)
-    lane_head = iota2((SEQ, GROUP), 1) // HEAD_DIM
-    step_raw = jnp.zeros((SEQ, GROUP), F32)
-    for h in range(4):
-        step_raw = jnp.where(lane_head == h, step_raw4[:, h : h + 1], step_raw)
+        return total, taps[3:4]
+
+    conv_i, conv_w, conv_r = old_taps(tapi_ref, bufi_ref), old_taps(tapw_ref, bufw_ref), old_taps(tapr_ref, bufr_ref)
     head_row = iota2((1, GROUP), 1) // HEAD_DIM
 
     def per_head(ref):
@@ -361,9 +342,32 @@
             wide = jnp.where(head_row == h, values[:, h : h + 1], wide)
         return wide
 
-    pre = step_raw + per_head(bias_ref)
+    bias_row, rate_row, skip_row = per_head(bias_ref), jnp.exp(per_head(rate_ref)), per_head(skip_ref)
+    ggain_row = as_row(ggain_ref)
+    wait_recv(recv_f.at[pl.ds(0, NT - 1)], r_t.at[1])
+    for k, dst in enumerate((wg2, wl2, wd2)):
+        forward_weights(3 + k, dst)
+    rows = dot(perm[...], recv_f[...].reshape(128, QW)).astype(BF16)
+    for q in range(4):
+        xrow[:, QW * q : QW * q + QW] = rows[32 * q : 32 * q + 32]
+    mixed_in = xrow[...]
+
+    def project(w):
+        return dot(mixed_in, w[...]).astype(BF16).astype(F32)
+
+    gate_z, input_new = project(pgv), project(piv)
+    write_new, read_new, step_raw4 = project(pwv), project(prv), dot_nt(mixed_in, psv[...]).astype(BF16).astype(F32)
+
+    xc = silu(conv_i[0] + input_new * conv_i[1])
+    bc = silu(conv_w[0] + write_new * conv_w[1])
+    rc = silu(conv_r[0] + read_new * conv_r[1])
+    lane_head = iota2((SEQ, GROUP), 1) // HEAD_DIM
+    step_raw = jnp.zeros((SEQ, GROUP), F32)
+    for h in range(4):
+        step_raw = jnp.where(lane_head == h, step_raw4[:, h : h + 1], step_raw)
+    pre = step_raw + bias_row
     step = jnp.maximum(pre, 0.0) + jnp.log1p(jnp.exp(-jnp.abs(pre)))
-    retain = jnp.exp(-step * jnp.exp(per_head(rate_ref)))
+    retain = jnp.exp(-step * rate_row)
     u = step * xc
     rcb = rc.astype(BF16)
     sub = iota2((8, GROUP), 0)
@@ -376,12 +380,12 @@
             acc = jnp.where(sub == j, got, acc)
         reads.append(acc)
     read = jnp.concatenate(reads, axis=0)
-    head = retain * read + u * jnp.sum(bc * rc, axis=1, keepdims=True) + per_head(skip_ref) * xc
+    head = retain * read + u * jnp.sum(bc * rc, axis=1, keepdims=True) + skip_row * xc
     gated = head.astype(BF16).astype(F32) * silu(gate_z)
-    gated = gated * lax.rsqrt(jnp.mean(gated * gated, axis=1, keepdims=True) + EPS) * as_row(ggain_ref)
+    gated = gated * lax.rsqrt(jnp.mean(gated * gated, axis=1, keepdims=True) + EPS) * ggain_row
     part = dot(gated.astype(BF16), pov[...]).astype(BF16)
     stacked = jnp.concatenate([part[:, QW * q : QW * q + QW] for q in range(4)], axis=0)
-    send_o[...] = dot(scatter_rows(NT), stacked).astype(BF16).reshape(NT, 16, QW)
+    send_o[...] = dot(permt[...], stacked).astype(BF16).reshape(NT, 16, QW)
     exchange_tp(lambda tt: send_o.at[tt], recv_o.at[t], 2)
     recv_o[t] = send_o[t]
     pltpu.make_async_copy(wg2.at[pl.ds(0, 3)], wg2.at[pl.ds(0, 3)], loc_sem.at[2]).wait()
@@ -459,9 +463,10 @@
             *[pltpu.VMEM((NT, hid_cols, 256), BF16), pltpu.VMEM((NT, hid_cols, 256), BF16), pltpu.VMEM((NT, hid_cols, 256), BF16)] * 2,
             pltpu.VMEM((NKV, 16, QW), BF16),
             pltpu.VMEM((NKV, 16, QW), BF16),
-            pltpu.VMEM((16 * NKV, 16 * NKV), BF16),
-            pltpu.VMEM((16 * NKV, 16 * NKV), BF16),
-            pltpu.VMEM((512, QW), BF16),
+            pltpu.VMEM((128, 128), BF16),
+            pltpu.VMEM((128, 128), BF16),
+            pltpu.VMEM((4, 128, QW), BF16),
+            pltpu.VMEM((4, 128, QW), BF16),
             pltpu.VMEM((NKV, 16, QW), BF16),
             pltpu.VMEM((NY, 16, QW), BF16),
             *[pltpu.VMEM((NZ, NY, 16, QW), BF16), pltpu.VMEM((2 * NY, 16, QW), BF16), pltpu.VMEM((NZ, 16, QW), BF16), pltpu.VMEM((NZ, 16, QW), BF16)] * 2,
@@ -481,9 +486,9 @@
             pltpu.VMEM((SEQ, GROUP, STATE), BF16),
             pltpu.VMEM((SEQ, D), BF16),
             pltpu.VMEM((32, QW), F32),
-            dma((10,)), dma((8,)), dma((4,)),
+            dma((10,)), dma((6,)), dma((4,)),
             dma((6,)), dma((6,)), dma((6,)), dma((6,)),
-            dma((2, 9)), dma((2, 6)), dma((2, 2)), dma((14,)), pltpu.SemaphoreType.REGULAR((2,)),
+            dma((9,)), dma((6,)), dma((2,)), dma((14,)), pltpu.SemaphoreType.REGULAR((2,)),
         ],
         compiler_params=pltpu.CompilerParams(
             collective_id=0, has_side_effects=True, vmem_limit_bytes=56 * 1024 * 1024

time: 74.6 us -> 72.7 us (0.975)
  Pallas kernels: 71.1 us -> 69.2 us
    pallas_call x1, Pallas kernels: 71.1 us -> 69.2 us  [per_device(): pl.pallas_call(kernel, out_shape=(pltpu.VMEM((SEQ, GROUP), BF16), pltpu.V...]
where the time goes in v4:
time: 72.7 us; the launch traced here: 72.5 us
  Pallas kernels  69.2 us (95%)
  local copies, waits for them, and re-layouts  2.62 us (4%)
    pallas_call x1, Pallas kernels, per_device(): pl.pallas_call(kernel, out_shape=(pltpu.VMEM((SEQ, GROUP), BF16), pltpu.V...  69.2 us
    unnamed x2, local copies, waits for them, and re-layouts  2.62 us

profile of v4, /device:TPU:1, one launch (start us, length us, event | category | flops | bytes accessed | tf_op | source)
XLA Modules:
  0.0 72.5 jit_solution(15520944215754693292)
XLA Ops:
  0.6 69.2 %layer.1 = (bf16[32,256]{1,0:T(8,128)(2,1)S(1)}, f32[32,256,128]{2,1,0:T(8,128)S(1)}) custom-call(bf16[32,256]{1,0:T(8,128)(2,1)} %refs_0_.1, bf16[2,128]{1,0:T(2,128)(2,1)} %bitcast.28, bf16[2,128]{1,0:T(2,128)(2,1)} %bitcast.29, bf16[16,128]{1,0:T(8,128)(2,1)} %bitcast.27, bf16[2,128]{1,0:T(2,128)(2,1)} %bitcast.30, f32[1,4]{1,0:T(1,128)} %bitcast.31, ...), custom_call_target="tpu_custom_call" | custom-call | tf_op jit(solution)/shard_map/layer/pallas_call | solution.py:451
  69.9 0.6 copy.31
  70.5 2.0 %copy.32 = f32[32,4,64,128]{3,2,1,0:T(8,128)} copy(f32[32,4,64,128]{3,2,1,0:T(8,128)S(1)} %bitcast.17) | data formatting | bytes 8388608

commit v5 on v4

--- a/solution.py
+++ b/solution.py
@@ -63,10 +63,10 @@
     res_ref, gain1_ref, gain2_ref, mgain_ref, ggain_ref, bias_ref, rate_ref, skip_ref = small[:8]
     tapi_ref, tapw_ref, tapr_ref, bufi_ref, bufw_ref, bufr_ref = small[8:]
     (
-        msg, recv_r, wg1, wl1, wd1, wg2, wl2, wd2,
+        msg, recv_r, up1, down1, up2, down2,
         ag1, ag2, perm, permt, lhs_v, hid, psend, znear, ry1, rn1, zs1, rz1, ry2, rn2, zs2, rz2,
         send_f, recv_f, recv_o, send_o, send_q, recv_q,
-        pgv, piv, pwv, prv, psv, pov, scan_f, scan_b, xrow, gsplit,
+        pgi, pwr, psv, pov, scan_f, scan_b, xrow, gsplit,
         loc_sem, s_all, r_t, s_w, r_wx, r_wo, r_wc, r_ag, r_y, r_z, in_sem, ready,
     ) = refs
     kv = lax.axis_index("kv")
@@ -110,8 +110,20 @@
         copy = pltpu.make_async_copy(small_in[k], small[k], in_sem.at[k])
         copy.start()
         l_small.append(copy)
-    for src, dst in ((fg_ref, wg1), (fl_ref, wl1), (fd_ref, wd1)):
-        local(src, dst.at[t], 1)
+    hid_units = fg_ref.shape[0]
+    sources = (fg_ref, fl_ref, fd_ref, sg_ref, sl_ref, sd_ref)
+    gathered = ((up1, 0), (up1, hid_units), (down1, 0), (up2, 0), (up2, hid_units), (down2, 0))
+
+    def block_of(k, s, first=0, rows=None):
+        dst, top = gathered[k]
+        return dst.at[pl.ds(top + first, rows or hid_units), pl.ds(pl.multiple_of(s * 256, 256), 256)]
+
+    def bytes_of(k, count):
+        dst, top = gathered[k]
+        return dst.at[pl.ds(top, hid_units), pl.ds(0, 256 * count)]
+
+    for k in range(3):
+        local(sources[k], block_of(k, t), 1)
     for k in range(3):
         l_small[k].wait()
 
@@ -141,42 +153,43 @@
 
     partner = t + 1 - 2 * core
     left, right, across = lax.rem(t + NT - 2, NT), lax.rem(t + 2, NT), lax.rem(t + 4, NT)
-    cuts = (fg_ref.shape[0], 0, 96)
-
-    def start_weights(k, src, dst):
+    cuts = (hid_units, 0, 96)
+
+    def start_weights(k):
         for tt in (right, left):
-            rcopy(src, dst.at[t], s_w.at[k], r_wx.at[k], (kv, tt)).start()
-        rcopy(src, dst.at[t], s_w.at[k], r_wc.at[k], (kv, partner)).start()
-
-    def relay_weights(k, dst):
-        wait_recv(dst.at[pl.ds(0, 2)], r_wx.at[k])
-        cut, depth = cuts[k % 3], dst.shape[1]
+            rcopy(sources[k], block_of(k, t), s_w.at[k], r_wx.at[k], (kv, tt)).start()
+        rcopy(sources[k], block_of(k, t), s_w.at[k], r_wc.at[k], (kv, partner)).start()
+
+    def relay_weights(k):
+        wait_recv(bytes_of(k, 2), r_wx.at[k])
+        cut = cuts[k % 3]
         if cut > 0:
-            part = dst.at[left, pl.ds(0, cut)]
+            part = block_of(k, left, 0, cut)
             rcopy(part, part, s_w.at[k], r_wo.at[k], (kv, right)).start()
-        if cut < depth:
-            part = dst.at[right, pl.ds(cut, depth - cut)]
+        if cut < hid_units:
+            part = block_of(k, right, cut, hid_units - cut)
             rcopy(part, part, s_w.at[k], r_wo.at[k], (kv, left)).start()
         for ss in (left, right):
-            rcopy(dst.at[ss], dst.at[ss], s_w.at[k], r_wc.at[k], (kv, partner)).start()
-
-    def forward_weights(k, dst):
-        wait_recv(dst.at[0], r_wo.at[k])
-        rcopy(dst.at[across], dst.at[across], s_w.at[k], r_wc.at[k], (kv, partner)).start()
-
-    def finish_weights(k, dst):
-        wait_recv(dst.at[pl.ds(0, 4)], r_wc.at[k])
-        wait_send(dst.at[pl.ds(0, 7)], s_w.at[k])
-
-    for k, (src, dst) in enumerate(((fg_ref, wg1), (fl_ref, wl1), (fd_ref, wd1))):
-        start_weights(k, src, dst)
+            rcopy(block_of(k, ss), block_of(k, ss), s_w.at[k], r_wc.at[k], (kv, partner)).start()
+
+    def forward_weights(k):
+        wait_recv(bytes_of(k, 1), r_wo.at[k])
+        rcopy(block_of(k, across), block_of(k, across), s_w.at[k], r_wc.at[k], (kv, partner)).start()
+
+    def finish_weights(k):
+        wait_recv(bytes_of(k, 4), r_wc.at[k])
+        wait_send(bytes_of(k, 7), s_w.at[k])
+
+    for k in range(3):
+        start_weights(k)
 
     l_mix = [
-        local(pg_ref, pgv, 3), local(pi_ref, piv, 4), local(pw_ref, pwv, 5), local(pr_ref, prv, 6),
+        local(pg_ref, pgi.at[:, pl.ds(0, 256)], 3), local(pi_ref, pgi.at[:, pl.ds(256, 256)], 4),
+        local(pw_ref, pwr.at[:, pl.ds(0, 128)], 5), local(pr_ref, pwr.at[:, pl.ds(128, 128)], 6),
         local(ps_ref, psv, 7), local(po_ref, pov, 8), local(scan_ref, scan_f, 9),
     ]
-    for src, dst in ((sg_ref, wg2), (sl_ref, wl2), (sd_ref, wd2)):
-        local(src, dst.at[t], 2)
+    for k in range(3, 6):
+        local(sources[k], block_of(k, t), 2)
 
     pl.semaphore_wait(ready.at[0], 2)
     for d in (2, 6):
@@ -198,7 +211,7 @@
     res1 = both[0:16]
     gsplit[...] = both[16:48]
 
-    ag_order = ((2, 0), (6, 0), (0, 1), (0, 3), (3, 0), (5, 0), (0, 2), (4, 0))
+    ag_order = ((2, 0), (6, 0), (3, 0), (5, 0), (0, 1), (0, 3), (4, 0), (0, 2))
 
     def gather_send(ag, slot, f, d, e, dev):
         k = ag_order.index((d, e)) if (d, e) in ag_order else 8
@@ -212,9 +225,9 @@
 
     def forward_gather(ag, f, between=()):
         for k, (d, e) in enumerate(ag_order):
-            for at, step, weights in between:
+            for at, step in between:
                 if at == k:
-                    relay_weights(step, weights)
+                    relay_weights(step)
             slot = lax.rem(z - d + NZ, NZ) * NY + lax.rem(y - e + NY, NY)
             wait_recv(ag.at[slot], r_ag.at[k])
             if e == 0:
@@ -228,25 +241,19 @@
         wait_recv(ag.at[pl.ds(0, 23)], r_ag.at[8])
         wait_send(ag.at[pl.ds(0, 31)], s_all.at[4])
 
-    def feed_forward(ag, wg, wl, wd, k):
+    def feed_forward(ag, up, down, k):
         for g in range(NKV // 8):
             rows = dot(perm[...], ag[8 * g : 8 * g + 8].reshape(128, QW)).astype(BF16)
             for q in range(4):
-                lhs_v[q, 32 * g : 32 * g + 32] = rows[32 * q : 32 * q + 32]
-        gate, lift = None, None
-        for s in range(NT):
-            q, h = s // 2, s % 2
-            part = lhs_v[q, :, 256 * h : 256 * h + 256]
-            g, u = dot_nt(part, wg[s]), dot_nt(part, wl[s])
-            gate = g if gate is None else gate + g
-            lift = u if lift is None else lift + u
-        finish_weights(k + 2, wd)
+                lhs_v[32 * g : 32 * g + 32, QW * q : QW * q + QW] = rows[32 * q : 32 * q + 32]
+        lhs = lhs_v[...]
+        gate, lift = dot_nt(lhs, up[0:hid_units]), dot_nt(lhs, up[hid_units : 2 * hid_units])
+        finish_weights(k + 2)
         hidden = (gate * jax.nn.sigmoid(gate) * lift).astype(BF16)
-        for s in range(NT):
-            q, h = s // 2, s % 2
-            out = dot(hidden, wd[s]).astype(BF16)
-            for g in range(NKV // 8):
-                hid[g, 32 * q : 32 * q + 32, 256 * h : 256 * h + 256] = out[32 * g : 32 * g + 32]
+        out = dot(hidden, down[...]).astype(BF16)
+        for g in range(NKV // 8):
+            for q in range(4):
+                hid[g, 32 * q : 32 * q + 32] = out[32 * g : 32 * g + 32, QW * q : QW * q + QW]
         for g in range(NKV // 8):
             psend[8 * g : 8 * g + 8] = dot(permt[...], hid[g]).astype(BF16).reshape(8, 16, QW)
 
@@ -286,9 +293,9 @@
                 near = psend[pl.ds(z * NY, NY)].astype(F32) + rn[0:NY].astype(F32) + rn[NY : 2 * NY].astype(F32)
                 znear[...] = near.astype(BF16)
                 reduce_send_y(lambda yy: znear.at[yy], ry, f, 0)
-            for at, step, weights in between:
+            for at, step in between:
                 if at == d:
-                    relay_weights(step, weights)
+                    relay_weights(step)
         own = with_y(znear[y].astype(F32), 0)
         wait_recv(rz.at[pl.ds(0, 5)], r_z.at[1])
         for d in (2, 6, 3, 5, 4):
@@ -298,21 +305,23 @@
 
     ag1[kv] = (res1 * piece_factor(res1) * gsplit[0:16]).astype(BF16)
     start_gather(ag1, 0)
-    forward_gather(ag1, 0, ((0, 0, wg1), (0, 1, wl1), (4, 2, wd1)))
-    for k, dst in enumerate((wg1, wl1, wd1)):
-        forward_weights(k, dst)
-    for k, (src, dst) in enumerate(((sg_ref, wg2), (sl_ref, wl2), (sd_ref, wd2))):
-        start_weights(3 + k, src, dst)
+    forward_gather(ag1, 0, ((0, 0), (0, 1), (4, 2)))
+    for k in range(3):
+        forward_weights(k)
+    for k in range(3, 6):
+        start_weights(k)
     finish_gather(ag1, 0)
-    pltpu.make_async_copy(wg1.at[pl.ds(0, 3)], wg1.at[pl.ds(0, 3)], loc_sem.at[1]).wait()
-    finish_weights(0, wg1)
-    finish_weights(1, wl1)
-    feed_forward(ag1, wg1, wl1, wd1, 0)
+    pltpu.make_async_copy(bytes_of(2, 3), bytes_of(2, 3), loc_sem.at[1]).wait()
+    finish_weights(0)
+    finish_weights(1)
+    feed_forward(ag1, up1, down1, 0)
     reduce_start(ry1, rn1, 0)
     for copy in l_mix:
         copy.wait()
-    scan_b[...] = scan_f[...].astype(BF16)
-    branch = reduce_finish(ry1, rn1, zs1, rz1, 0, ((4, 3, wg2), (4, 4, wl2), (5, 5, wd2)))
+    for k in range(2):
+        for j in range(SEQ // 2):
+            scan_b[j, :, STATE * k : STATE * k + STATE] = scan_f[2 * j + k].astype(BF16)
+    branch = reduce_finish(ry1, rn1, zs1, rz1, 0, ((4, 3), (4, 4), (5, 5)))
     first = (res1 + 0.5 * branch).astype(BF16).astype(F32)
 
     row, col = iota2((16, 16), 0), iota2((16, 16), 1)
@@ -345,8 +354,8 @@
     bias_row, rate_row, skip_row = per_head(bias_ref), jnp.exp(per_head(rate_ref)), per_head(skip_ref)
     ggain_row = as_row(ggain_ref)
     wait_recv(recv_f.at[pl.ds(0, NT - 1)], r_t.at[1])
-    for k, dst in enumerate((wg2, wl2, wd2)):
-        forward_weights(3 + k, dst)
+    for k in range(3, 6):
+        forward_weights(k)
     rows = dot(perm[...], recv_f[...].reshape(128, QW)).astype(BF16)
     for q in range(4):
         xrow[:, QW * q : QW * q + QW] = rows[32 * q : 32 * q + 32]
@@ -355,9 +364,10 @@
     def project(w):
         return dot(mixed_in, w[...]).astype(BF16).astype(F32)
 
-    gate_z, input_new = project(pgv), project(piv)
-    write_new, read_new, step_raw4 = project(pwv), project(prv), dot_nt(mixed_in, psv[...]).astype(BF16).astype(F32)
-
+    wide, narrow = project(pgi), project(pwr)
+    gate_z, input_new = wide[:, :GROUP], wide[:, GROUP:]
+    write_new, read_new = narrow[:, :STATE], narrow[:, STATE:]
+    step_raw4 = dot_nt(mixed_in, psv[...]).astype(BF16).astype(F32)
     xc = silu(conv_i[0] + input_new * conv_i[1])
     bc = silu(conv_w[0] + write_new * conv_w[1])
     rc = silu(conv_r[0] + read_new * conv_r[1])
@@ -369,15 +379,14 @@
     step = jnp.maximum(pre, 0.0) + jnp.log1p(jnp.exp(-jnp.abs(pre)))
     retain = jnp.exp(-step * rate_row)
     u = step * xc
-    rcb = rc.astype(BF16)
-    sub = iota2((8, GROUP), 0)
+    rc_pair = jnp.concatenate([rc, rc], axis=1)
+    sub, half = iota2((8, 2 * STATE), 0), iota2((8, 2 * STATE), 1) // STATE
     reads = []
     for g in range(4):
         acc = jnp.zeros((8, GROUP), F32)
-        for j in range(8):
-            b = 8 * g + j
-            got = dot_nt(rcb[8 * g : 8 * g + 8], scan_b[b])
-            acc = jnp.where(sub == j, got, acc)
+        for j in range(4):
+            row = jnp.where(sub == 2 * j + half, rc_pair[8 * g : 8 * g + 8], 0.0).astype(BF16)
+            acc = acc + dot_nt(row, scan_b[4 * g + j])
         reads.append(acc)
     read = jnp.concatenate(reads, axis=0)
     head = retain * read + u * jnp.sum(bc * rc, axis=1, keepdims=True) + skip_row * xc
@@ -388,7 +397,7 @@
     send_o[...] = dot(permt[...], stacked).astype(BF16).reshape(NT, 16, QW)
     exchange_tp(lambda tt: send_o.at[tt], recv_o.at[t], 2)
     recv_o[t] = send_o[t]
-    pltpu.make_async_copy(wg2.at[pl.ds(0, 3)], wg2.at[pl.ds(0, 3)], loc_sem.at[2]).wait()
+    pltpu.make_async_copy(bytes_of(5, 3), bytes_of(5, 3), loc_sem.at[2]).wait()
     u_cols = jnp.transpose(u)
     for b in range(SEQ):
         for h in range(4):
@@ -406,9 +415,9 @@
     start_gather(ag2, 1)
     forward_gather(ag2, 1)
     finish_gather(ag2, 1)
-    finish_weights(3, wg2)
-    finish_weights(4, wl2)
-    feed_forward(ag2, wg2, wl2, wd2, 3)
+    finish_weights(3)
+    finish_weights(4)
+    feed_forward(ag2, up2, down2, 3)
     reduce_start(ry2, rn2, 1)
     branch = reduce_finish(ry2, rn2, zs2, rz2, 1)
     final = (res2 + 0.5 * branch).astype(BF16)
@@ -460,12 +469,12 @@
             *[pltpu.VMEM(a.shape, a.dtype) for a in small],
             pltpu.VMEM((NT, 16, GROUP), BF16),
             pltpu.VMEM((NT, 16, GROUP), BF16),
-            *[pltpu.VMEM((NT, hid_cols, 256), BF16), pltpu.VMEM((NT, hid_cols, 256), BF16), pltpu.VMEM((NT, hid_cols, 256), BF16)] * 2,
+            *[pltpu.VMEM((2 * hid_cols, D), BF16), pltpu.VMEM((hid_cols, D), BF16)] * 2,
             pltpu.VMEM((NKV, 16, QW), BF16),
             pltpu.VMEM((NKV, 16, QW), BF16),
             pltpu.VMEM((128, 128), BF16),
             pltpu.VMEM((128, 128), BF16),
-            pltpu.VMEM((4, 128, QW), BF16),
+            pltpu.VMEM((128, D), BF16),
             pltpu.VMEM((4, 128, QW), BF16),
             pltpu.VMEM((NKV, 16, QW), BF16),
             pltpu.VMEM((NY, 16, QW), BF16),
@@ -476,14 +485,12 @@
             pltpu.VMEM((NT, 16, QW), BF16),
             pltpu.VMEM((NT, 16, GROUP), BF16),
             pltpu.VMEM((NT, 16, GROUP), BF16),
+            pltpu.VMEM((D, 512), BF16),
             pltpu.VMEM((D, 256), BF16),
-            pltpu.VMEM((D, 256), BF16),
-            pltpu.VMEM((D, 128), BF16),
-            pltpu.VMEM((D, 128), BF16),
             pltpu.VMEM((4, D), BF16),
             pltpu.VMEM((256, D), BF16),
             pltpu.VMEM((SEQ, GROUP, STATE), F32),
-            pltpu.VMEM((SEQ, GROUP, STATE), BF16),
+            pltpu.VMEM((SEQ // 2, GROUP, 2 * STATE), BF16),
             pltpu.VMEM((SEQ, D), BF16),
             pltpu.VMEM((32, QW), F32),
             dma((10,)), dma((6,)), dma((4,)),

time: 72.7 us -> 72.5 us (level)
  no operation moved by 1% of the time
where the time goes in v5:
time: 72.5 us; the launch traced here: 72.3 us
  Pallas kernels  69 us (95%)
  local copies, waits for them, and re-layouts  2.62 us (4%)
    pallas_call x1, Pallas kernels, per_device(): pl.pallas_call(kernel, out_shape=(pltpu.VMEM((SEQ, GROUP), BF16), pltpu.V...  69 us
    unnamed x2, local copies, waits for them, and re-layouts  2.62 us

profile of v5, /device:TPU:1, one launch (start us, length us, event | category | flops | bytes accessed | tf_op | source)
XLA Modules:
  0.0 72.3 jit_solution(17666979057009433856)
XLA Ops:
  0.6 69.0 %layer.1 = (bf16[32,256]{1,0:T(8,128)(2,1)S(1)}, f32[32,256,128]{2,1,0:T(8,128)S(1)}) custom-call(bf16[32,256]{1,0:T(8,128)(2,1)} %refs_0_.1, bf16[2,128]{1,0:T(2,128)(2,1)} %bitcast.28, bf16[2,128]{1,0:T(2,128)(2,1)} %bitcast.29, bf16[16,128]{1,0:T(8,128)(2,1)} %bitcast.27, bf16[2,128]{1,0:T(2,128)(2,1)} %bitcast.30, f32[1,4]{1,0:T(1,128)} %bitcast.31, ...), custom_call_target="tpu_custom_call" | custom-call | tf_op jit(solution)/shard_map/layer/pallas_call | solution.py:460
  69.7 0.6 copy.31
  70.3 2.0 %copy.32 = f32[32,4,64,128]{3,2,1,0:T(8,128)} copy(f32[32,4,64,128]{3,2,1,0:T(8,128)S(1)} %bitcast.17) | data formatting | bytes 8388608

commit v6 on v5

--- a/solution.py
+++ b/solution.py
@@ -119,8 +119,8 @@
         return dst.at[pl.ds(top + first, rows or hid_units), pl.ds(pl.multiple_of(s * 256, 256), 256)]
 
     def bytes_of(k, count):
-        dst, top = gathered[k]
-        return dst.at[pl.ds(top, hid_units), pl.ds(0, 256 * count)]
+        dst = gathered[k][0]
+        return dst.at[:, pl.ds(0, 256 * count)]
 
     for k in range(3):
         local(sources[k], block_of(k, t), 1)
@@ -155,30 +155,38 @@
     left, right, across = lax.rem(t + NT - 2, NT), lax.rem(t + 2, NT), lax.rem(t + 4, NT)
     cuts = (hid_units, 0, 96)
 
+    def sem_of(k):
+        return 2 * (k // 3) + (k % 3) // 2
+
     def start_weights(k):
         for tt in (right, left):
-            rcopy(sources[k], block_of(k, t), s_w.at[k], r_wx.at[k], (kv, tt)).start()
-        rcopy(sources[k], block_of(k, t), s_w.at[k], r_wc.at[k], (kv, partner)).start()
+            rcopy(sources[k], block_of(k, t), s_w.at[sem_of(k)], r_wx.at[sem_of(k)], (kv, tt)).start()
+        rcopy(sources[k], block_of(k, t), s_w.at[sem_of(k)], r_wc.at[sem_of(k)], (kv, partner)).start()
 
     def relay_weights(k):
-        wait_recv(bytes_of(k, 2), r_wx.at[k])
+        if k % 3 != 1:
+            wait_recv(bytes_of(k, 2), r_wx.at[sem_of(k)])
         cut = cuts[k % 3]
         if cut > 0:
             part = block_of(k, left, 0, cut)
-            rcopy(part, part, s_w.at[k], r_wo.at[k], (kv, right)).start()
+            rcopy(part, part, s_w.at[sem_of(k)], r_wo.at[sem_of(k)], (kv, right)).start()
         if cut < hid_units:
             part = block_of(k, right, cut, hid_units - cut)
-            rcopy(part, part, s_w.at[k], r_wo.at[k], (kv, left)).start()
+            rcopy(part, part, s_w.at[sem_of(k)], r_wo.at[sem_of(k)], (kv, left)).start()
         for ss in (left, right):
-            rcopy(block_of(k, ss), block_of(k, ss), s_w.at[k], r_wc.at[k], (kv, partner)).start()
+            rcopy(block_of(k, ss), block_of(k, ss), s_w.at[sem_of(k)], r_wc.at[sem_of(k)], (kv, partner)).start()
 
     def forward_weights(k):
-        wait_recv(bytes_of(k, 1), r_wo.at[k])
-        rcopy(block_of(k, across), block_of(k, across), s_w.at[k], r_wc.at[k], (kv, partner)).start()
+        if k % 3 != 1:
+            wait_recv(bytes_of(k, 1), r_wo.at[sem_of(k)])
+        rcopy(block_of(k, across), block_of(k, across), s_w.at[sem_of(k)], r_wc.at[sem_of(k)], (kv, partner)).start()
 
     def finish_weights(k):
-        wait_recv(bytes_of(k, 4), r_wc.at[k])
-        wait_send(bytes_of(k, 7), s_w.at[k])
+        if k % 3 != 1:
+            wait_recv(bytes_of(k, 4), r_wc.at[sem_of(k)])
+
+    def sent_weights(k):
+        wait_send(bytes_of(k, 7), s_w.at[sem_of(k)])
 
     for k in range(3):
         start_weights(k)
@@ -239,7 +247,6 @@
 
     def finish_gather(ag, f):
         wait_recv(ag.at[pl.ds(0, 23)], r_ag.at[8])
-        wait_send(ag.at[pl.ds(0, 31)], s_all.at[4])
 
     def feed_forward(ag, up, down, k):
         for g in range(NKV // 8):
@@ -300,7 +307,6 @@
         wait_recv(rz.at[pl.ds(0, 5)], r_z.at[1])
         for d in (2, 6, 3, 5, 4):
             own = own + rz[d].astype(F32)
-        wait_send(psend.at[pl.ds(0, 31)], s_all.at[5])
         return own
 
     ag1[kv] = (res1 * piece_factor(res1) * gsplit[0:16]).astype(BF16)
@@ -316,6 +322,9 @@
     finish_weights(1)
     feed_forward(ag1, up1, down1, 0)
     reduce_start(ry1, rn1, 0)
+    wait_send(ag1.at[pl.ds(0, 31)], s_all.at[4])
+    sent_weights(0)
+    sent_weights(2)
     for copy in l_mix:
         copy.wait()
     for k in range(2):
@@ -331,6 +340,7 @@
     send_f[...] = (first * piece_factor(first) * mixer_gain).astype(BF16)
     exchange_tp(lambda tt: send_f, recv_f.at[t], 1)
     recv_f[t] = send_f[...]
+    wait_send(psend.at[pl.ds(0, 31)], s_all.at[5])
     def silu(v):
         return v * jax.nn.sigmoid(v)
 
@@ -354,8 +364,6 @@
     bias_row, rate_row, skip_row = per_head(bias_ref), jnp.exp(per_head(rate_ref)), per_head(skip_ref)
     ggain_row = as_row(ggain_ref)
     wait_recv(recv_f.at[pl.ds(0, NT - 1)], r_t.at[1])
-    for k in range(3, 6):
-        forward_weights(k)
     rows = dot(perm[...], recv_f[...].reshape(128, QW)).astype(BF16)
     for q in range(4):
         xrow[:, QW * q : QW * q + QW] = rows[32 * q : 32 * q + 32]
@@ -397,6 +405,8 @@
     send_o[...] = dot(permt[...], stacked).astype(BF16).reshape(NT, 16, QW)
     exchange_tp(lambda tt: send_o.at[tt], recv_o.at[t], 2)
     recv_o[t] = send_o[t]
+    for k in range(3, 6):
+        forward_weights(k)
     pltpu.make_async_copy(bytes_of(5, 3), bytes_of(5, 3), loc_sem.at[2]).wait()
     u_cols = jnp.transpose(u)
     for b in range(SEQ):
@@ -435,6 +445,10 @@
     wait_recv(recv_q.at[pl.ds(0, NT - 1)], r_t.at[3])
     out_ref[...] = dot(pick32, recv_q[...].reshape(128, 256)).astype(BF16)
 
+    wait_send(ag2.at[pl.ds(0, 31)], s_all.at[4])
+    wait_send(psend.at[pl.ds(0, 31)], s_all.at[5])
+    sent_weights(3)
+    sent_weights(5)
     l_state.wait()
     for k, block in enumerate((recv_r, recv_f, recv_o, recv_q)):
         wait_send(block.at[pl.ds(0, NT - 1)], s_all.at[k])
@@ -494,7 +508,7 @@
             pltpu.VMEM((SEQ, D), BF16),
             pltpu.VMEM((32, QW), F32),
             dma((10,)), dma((6,)), dma((4,)),
-            dma((6,)), dma((6,)), dma((6,)), dma((6,)),
+            dma((4,)), dma((4,)), dma((4,)), dma((4,)),
             dma((9,)), dma((6,)), dma((2,)), dma((14,)), pltpu.SemaphoreType.REGULAR((2,)),
         ],
         compiler_params=pltpu.CompilerParams(

time: 72.5 us -> 72.5 us (level)
  no operation moved by 1% of the time
where the time goes in v6:
time: 72.5 us; the launch traced here: 72.3 us
  Pallas kernels  69 us (95%)
  local copies, waits for them, and re-layouts  2.62 us (4%)
    pallas_call x1, Pallas kernels, per_device(): pl.pallas_call(kernel, out_shape=(pltpu.VMEM((SEQ, GROUP), BF16), pltpu.V...  69 us
    unnamed x2, local copies, waits for them, and re-layouts  2.62 us

profile of v6, /device:TPU:1, one launch (start us, length us, event | category | flops | bytes accessed | tf_op | source)
XLA Modules:
  0.0 72.3 jit_solution(8330106526274890003)
XLA Ops:
  0.6 69.0 %layer.1 = (bf16[32,256]{1,0:T(8,128)(2,1)S(1)}, f32[32,256,128]{2,1,0:T(8,128)S(1)}) custom-call(bf16[32,256]{1,0:T(8,128)(2,1)} %refs_0_.1, bf16[2,128]{1,0:T(2,128)(2,1)} %bitcast.28, bf16[2,128]{1,0:T(2,128)(2,1)} %bitcast.29, bf16[16,128]{1,0:T(8,128)(2,1)} %bitcast.27, bf16[2,128]{1,0:T(2,128)(2,1)} %bitcast.30, f32[1,4]{1,0:T(1,128)} %bitcast.31, ...), custom_call_target="tpu_custom_call" | custom-call | tf_op jit(solution)/shard_map/layer/pallas_call | solution.py:474
  69.7 0.6 copy.31
  70.3 2.0 %copy.32 = f32[32,4,64,128]{3,2,1,0:T(8,128)} copy(f32[32,4,64,128]{3,2,1,0:T(8,128)S(1)} %bitcast.17) | data formatting | bytes 8388608
